TPU v7x, 32 devices: a whole 2x2x4 slice. The times are simulated.
32 devices in a mesh: sp: 8 (over z, x), tp: 4 (over y, core).
Axes of the slice: x: 2, y: 2, z: 4, core: 2. Of those that a mesh axis runs over, the one named last changes fastest.
Arguments:
- queries: bfloat16 [3072, 768], P('sp', 'tp'), may hold values from -8 to 8
- keys: bfloat16 [3072, 256], P('sp', 'tp'), may hold values from -8 to 8
- values: bfloat16 [3072, 256], P('sp', 'tp'), may hold values from -6 to 6
- sinks: float32 [12], P('tp'), may hold values from 1 to 6
- residual: bfloat16 [3072, 2048], P('sp'), may hold values from -6 to 6
- out_weight: bfloat16 [768, 2048], replicated, may hold values from -3 to 3
- norm_gain: float32 [2048], replicated, may hold values from 0.1 to 1.9
- shared_gate: bfloat16 [2048, 512], P(None, 'tp'), may hold values from -0.125 to 0.125
- shared_up: bfloat16 [2048, 512], P(None, 'tp'), may hold values from -0.125 to 0.125
- shared_down: bfloat16 [512, 2048], P('tp'), may hold values from -0.25 to 0.25
- expert_ids: int32 [3072, 2], P('sp'), may hold values from 0 to 15, all different within a row; in each aligned block of 96 rows (0 to 95, 96 to 191, ...) at most 24 rows name the same one
- route_weights: float32 [3072, 2], P(('sp', 'tp')), may hold values from 0.2 to 2
- expert_gate: bfloat16 [16, 2048, 1024], P('sp', None, 'tp'), may hold values from -0.125 to 0.125
- expert_up: bfloat16 [16, 2048, 1024], P('sp', None, 'tp'), may hold values from -0.125 to 0.125
- expert_down: bfloat16 [16, 1024, 2048], P('sp', 'tp'), may hold values from -0.1875 to 0.1875
Outputs:
- layer_out: bfloat16 [3072, 2048], P(('sp', 'tp'))
Inputs may be any that keep to these rules, and one draw needn't show every extreme that they name: `expert_ids`: each row names 2 different experts. In each aligned block of 96 rows no expert is named more than 24 times, a bound that some blocks reach.
All inputs are finite; a program needn't handle non-finite values.
Results may differ from a plain program's by a relative error of at most 0.018.
Values may be sent and summed in bfloat16 or wider, within the bound.
No kernel may reach another device: no remote copies, remote signals or barrier semaphores. Data moves between devices by JAX's collectives and lax.ppermute only.
A program may use at most 128 MiB of HBM per device.

v0:
```python
import functools

import jax
import jax.numpy as jnp
import numpy as np
from jax import lax
from jax.experimental import pallas as pl
from jax.experimental.pallas import tpu as pltpu
from jax.sharding import PartitionSpec as P

HEAD_DIM = 64
WINDOW = 128
GRID_W = 64
TOPK = 2
ROPE_BASE = 10000.0
NEG_LARGE = -1e30
NORM_EPSILON = 1e-06

BF = jnp.bfloat16
F32 = jnp.float32
VMEM_LIMIT = 56 * 1024 * 1024


def dot32(a, b):
    return jnp.dot(a, b, preferred_element_type=F32)


def call(body, outs, operands, scalars=(), scratch=(), own=(), flops=0, moved=0):
    whole = lambda shape: pl.BlockSpec(shape, lambda i, *s: (0,) * len(shape))
    specs = [whole(x.shape) for x in operands]
    for at, rows, which in own:
        index = lambda i, *s, which=which: (s[0][which], 0)
        specs[at] = pl.BlockSpec((rows, operands[at].shape[1]), index)
    operands = tuple(operands)
    grid_spec = pltpu.PrefetchScalarGridSpec(
        num_scalar_prefetch=len(scalars),
        grid=(1,),
        in_specs=specs,
        out_specs=[whole(shape) for shape, kind in outs],
        scratch_shapes=list(scratch),
    )
    return pl.pallas_call(
        body,
        out_shape=[jax.ShapeDtypeStruct(shape, kind) for shape, kind in outs],
        grid_spec=grid_spec,
        compiler_params=pltpu.CompilerParams(vmem_limit_bytes=VMEM_LIMIT),
        cost_estimate=pl.CostEstimate(flops=flops, bytes_accessed=moved, transcendentals=0),
    )(*scalars, *operands)


def attention_body(
    first_ref, sink_ref, q_ref, k_ref, v_ref, before_ref, after_ref, spectrum_ref,
    out_ref, keys_ref, values_ref, total_rows,
):
    key_width, rows = k_ref.shape
    key_heads = key_width // HEAD_DIM
    group = q_ref.shape[0] // key_width
    wide = rows + 2 * WINDOW
    quarter = HEAD_DIM // 4
    first_row = first_ref[0] * rows
    place = lax.broadcasted_iota(jnp.int32, (2 * quarter, wide), 1) + (first_row - WINDOW)
    lane_row = lax.broadcasted_iota(jnp.int32, (2 * quarter, wide), 0)
    shift = GRID_W.bit_length() - 1
    at = jnp.where(
        lane_row < quarter, lax.shift_right_arithmetic(place, shift), place & (GRID_W - 1)
    )
    angles = at.astype(F32) * spectrum_ref[...]
    cosine, sine = jnp.cos(angles), jnp.sin(angles)

    def turn(x, start):
        u = x.astype(F32)
        end = start + x.shape[1]
        pieces = []
        for half in range(2):
            c = cosine[half * quarter : (half + 1) * quarter, start:end]
            s = sine[half * quarter : (half + 1) * quarter, start:end]
            former = u[2 * half * quarter : (2 * half + 1) * quarter]
            latter = u[(2 * half + 1) * quarter : (2 * half + 2) * quarter]
            pieces.append(former * c - latter * s)
            pieces.append(former * s + latter * c)
        return jnp.concatenate(pieces, axis=0)

    query_index = lax.broadcasted_iota(jnp.int32, (3 * WINDOW, WINDOW), 1)
    key_index = lax.broadcasted_iota(jnp.int32, (3 * WINDOW, WINDOW), 0)
    apart = key_index - query_index
    near = (apart >= 0) & (apart <= 2 * WINDOW)
    blocks = rows // WINDOW
    finished = [[] for _ in range(blocks)]
    for g in range(key_heads):
        cut = slice(g * HEAD_DIM, (g + 1) * HEAD_DIM)
        late = slice(key_width + g * HEAD_DIM, key_width + (g + 1) * HEAD_DIM)
        keys = jnp.concatenate([before_ref[cut], k_ref[cut], after_ref[cut]], axis=1)
        keys_ref[...] = turn(keys, 0).T.astype(BF)
        values_ref[...] = jnp.concatenate([before_ref[late], v_ref[cut], after_ref[late]], axis=1)
        turned = [
            turn(q_ref[h * HEAD_DIM : (h + 1) * HEAD_DIM], WINDOW).astype(BF)
            for h in range(g * group, (g + 1) * group)
        ]
        sink = jnp.concatenate(
            [jnp.full((1, WINDOW), sink_ref[h], F32) for h in range(g * group, (g + 1) * group)],
            axis=1,
        )
        for b in range(blocks):
            key_at = key_index + (first_row + (b - 1) * WINDOW)
            allowed = near & (key_at >= 0) & (key_at < total_rows)
            penalty = jnp.where(allowed, 0.0, NEG_LARGE)
            penalty = jnp.concatenate([penalty] * group, axis=1)
            heads = jnp.concatenate(
                [q[:, b * WINDOW : (b + 1) * WINDOW] for q in turned], axis=1
            )
            scores = dot32(keys_ref[b * WINDOW : (b + 3) * WINDOW], heads)
            scores = scores * HEAD_DIM ** (-0.5) + penalty
            highest = jnp.maximum(jnp.max(scores, axis=0, keepdims=True), sink)
            lifted = jnp.exp(scores - highest)
            denominator = jnp.sum(lifted, axis=0, keepdims=True) + jnp.exp(sink - highest)
            probabilities = (lifted * (1.0 / denominator)).astype(BF)
            result = dot32(values_ref[:, b * WINDOW : (b + 3) * WINDOW], probabilities)
            for i in range(group):
                finished[b].append(result[:, i * WINDOW : (i + 1) * WINDOW].T.astype(BF))
    for b in range(blocks):
        out_ref[b * WINDOW : (b + 1) * WINDOW, :] = jnp.concatenate(finished[b], axis=1)


def mixed_and_normed(residual, parts, weight, gain):
    mixed = (residual.astype(F32) + dot32(parts, weight)).astype(BF)
    wide = mixed.astype(F32)
    scale = lax.rsqrt(jnp.mean(wide * wide, axis=1, keepdims=True) + NORM_EPSILON)
    return mixed, (wide * scale * gain).astype(BF)


def ranks_of(ids_ref, block, experts):
    own = ids_ref.shape[2]
    expert_index = lax.broadcasted_iota(jnp.int32, (experts, own), 0)
    ids = ids_ref[block]
    named = expert_index == ids[0:1, :]
    for k in range(1, ids.shape[0]):
        named = named | (expert_index == ids[k : k + 1, :])
    ones = jnp.where(named, 1.0, 0.0).astype(BF)
    earlier = jnp.where(
        lax.broadcasted_iota(jnp.int32, (own, own), 0)
        < lax.broadcasted_iota(jnp.int32, (own, own), 1),
        1.0,
        0.0,
    ).astype(BF)
    return jnp.where(named, dot32(ones, earlier), -1.0).astype(BF)


def slot_choice(ranks, place, rank, turn, experts_here, c):
    experts = ranks.shape[0]
    wanted = (place ^ turn) * experts_here + c
    shape = (place.shape[0], experts)
    pick = jnp.where(lax.broadcasted_iota(jnp.int32, shape, 1) == wanted, 1.0, 0.0).astype(BF)
    return jnp.where(dot32(pick, ranks) == rank, 1.0, 0.0).astype(BF)


def dispatch_body(
    order_ref, parts_ref, residual_ref, weight_ref, gain_ref, ids_ref, place_ref, rank_ref,
    mixed_ref, slot_ref, experts,
):
    own = mixed_ref.shape[0]
    start = pl.multiple_of(order_ref[0] * own, 16)
    parts = [parts_ref[j, pl.ds(start, own), :] for j in range(parts_ref.shape[0])]
    parts = jnp.concatenate(parts, axis=1)
    mixed, normed = mixed_and_normed(residual_ref[...], parts, weight_ref[...], gain_ref[...])
    mixed_ref[...] = mixed
    ranks = ranks_of(ids_ref, order_ref[0], experts[0])
    chosen = slot_choice(ranks, place_ref[...], rank_ref[...], 0, experts[1], 0)
    slot_ref[...] = dot32(chosen, normed).astype(BF)


def gated(x, gate, up):
    gate_values = dot32(x, gate)
    up_values = dot32(x, up)
    return (gate_values / (1.0 + jnp.exp(-gate_values)) * up_values).astype(BF)


def second_body(
    order_ref, turn_ref, parts_ref, near_ref, far_ref, weight_ref, gain_ref, ids_ref,
    place_ref, rank_ref, *slot_refs, experts,
):
    ways = parts_ref.shape[0]
    own = near_ref.shape[0]
    blocks = []
    for m in range(0, ways, 2):
        start = pl.multiple_of(order_ref[m] * own, 16)
        parts = [parts_ref[j, pl.ds(start, own), :] for j in range(ways)]
        blocks.append(jnp.concatenate(parts, axis=1))
    residual = jnp.concatenate([near_ref[...], far_ref[...]], axis=0)
    _, normed = mixed_and_normed(
        residual, jnp.concatenate(blocks, axis=0), weight_ref[...], gain_ref[...]
    )
    pieces = len(slot_refs) // (experts[1] - 1)
    for m in range(0, ways, 2):
        ranks = ranks_of(ids_ref, order_ref[m], experts[0])
        rows = normed[(m // 2) * own : (m // 2 + 1) * own]
        for c in range(1, experts[1]):
            chosen = slot_choice(
                ranks, place_ref[...], rank_ref[...], turn_ref[0], experts[1], c
            )
            result = dot32(chosen, rows)
            for p in range(pieces):
                slots_ref = slot_refs[(c - 1) * pieces + p]
                count = slots_ref.shape[0] // (ways // 2)
                slots_ref[(m // 2) * count : (m // 2 + 1) * count] = result[
                    p * count : (p + 1) * count
                ].astype(BF)


def shared_body(
    order_ref, parts_ref, residual_ref, weight_ref, gain_ref, gate_ref, up_ref, down_ref,
    keep_ref, send_ref, scratch_ref,
):
    ways = parts_ref.shape[0]
    own = keep_ref.shape[1]
    parts = jnp.concatenate([parts_ref[j] for j in range(ways)], axis=1)
    _, normed = mixed_and_normed(
        residual_ref[...], parts, weight_ref[...], gain_ref[...]
    )
    hidden = gated(normed, gate_ref[...], up_ref[...])
    scratch_ref[...] = dot32(hidden, down_ref[...]).astype(BF)
    for m in range(ways):
        start = pl.multiple_of(order_ref[m] * own, 16)
        target = keep_ref if m % 2 == 0 else send_ref
        target[m // 2] = scratch_ref[pl.ds(start, own), :]


def expert_body(c, count, *refs):
    xs, (gate_hbm, up_hbm, down_hbm) = refs[:count], refs[count : count + 3]
    outs = refs[count + 3 : 2 * count + 3]
    x_buf, gate, up, down, out_buf, sems = refs[2 * count + 3 :]
    loads = [
        pltpu.make_async_copy(gate_hbm.at[c], gate, sems.at[0]),
        pltpu.make_async_copy(up_hbm.at[c], up, sems.at[1]),
        pltpu.make_async_copy(down_hbm.at[c], down, sems.at[2]),
    ]
    reads = [
        pltpu.make_async_copy(xs[i], x_buf.at[i], sems.at[3 + i]) for i in range(count)
    ]
    writes = [
        pltpu.make_async_copy(out_buf.at[i], outs[i], sems.at[3 + count + i])
        for i in range(count)
    ]
    reads[0].start()
    loads[0].start()
    loads[1].start()
    loads[2].start()
    for i in range(1, count):
        reads[i].start()
    reads[0].wait()
    loads[0].wait()
    for i in range(count):
        if i:
            reads[i].wait()
        gate_values = dot32(x_buf[i], gate[...])
        if i == 0:
            loads[1].wait()
        up_values = dot32(x_buf[i], up[...])
        hidden = (gate_values / (1.0 + jnp.exp(-gate_values)) * up_values).astype(BF)
        if i == 0:
            loads[2].wait()
        out_buf[i] = dot32(hidden, down[...]).astype(BF)
        writes[i].start()
    for i in range(count):
        writes[i].wait()


def expert_rows(c, xs, gates, ups, downs):
    rows, width = xs[0].shape
    hid = gates.shape[2]
    count = len(xs)
    hbm = pl.BlockSpec(memory_space=pltpu.HBM)
    return pl.pallas_call(
        functools.partial(expert_body, c, count),
        out_shape=[jax.ShapeDtypeStruct((rows, width), BF)] * count,
        in_specs=[hbm] * (count + 3),
        out_specs=[hbm] * count,
        scratch_shapes=[
            pltpu.VMEM((count, rows, width), BF),
            pltpu.VMEM((width, hid), BF),
            pltpu.VMEM((width, hid), BF),
            pltpu.VMEM((hid, width), BF),
            pltpu.VMEM((count, rows, width), BF),
            pltpu.SemaphoreType.DMA((3 + 2 * count,)),
        ],
        compiler_params=pltpu.CompilerParams(vmem_limit_bytes=VMEM_LIMIT),
        cost_estimate=pl.CostEstimate(
            flops=6 * rows * width * hid * count,
            bytes_accessed=4 * rows * width * count + 6 * width * hid,
            transcendentals=0,
        ),
    )(*xs, gates, ups, downs)


def joined_body(count, *refs):
    pieces, outs = refs[:count], refs[count:]
    rows = outs[0].shape[0] // count
    for p, piece in enumerate(pieces):
        for h, out in enumerate(outs):
            out[p * rows : (p + 1) * rows] = piece[h * rows : (h + 1) * rows]


def joined(pieces, halves):
    rows, width = pieces[0].shape
    count = len(pieces)
    return call(
        functools.partial(joined_body, count),
        [((count * rows // halves, width), BF)] * halves,
        pieces,
        flops=rows * width * count,
        moved=4 * rows * width * count,
    )


def prepare_body(
    order_ref, turn_ref, ids_ref, route_ref, place_ref, rank_ref, out_ref, experts,
):
    own = ids_ref.shape[0]
    expert_index = lax.broadcasted_iota(jnp.int32, (own, experts[0]), 1)
    weight = jnp.zeros((own, experts[0]), F32)
    named = expert_index < 0
    for k in range(ids_ref.shape[1]):
        match = expert_index == ids_ref[:, k : k + 1]
        named = named | match
        weight = weight + jnp.where(match, route_ref[:, k : k + 1], 0.0)
    ones = jnp.where(named, 1.0, 0.0).astype(BF)
    earlier = jnp.where(
        lax.broadcasted_iota(jnp.int32, (own, own), 1)
        < lax.broadcasted_iota(jnp.int32, (own, own), 0),
        1.0,
        0.0,
    ).astype(BF)
    ranks = jnp.where(named, dot32(earlier, ones), -1.0).astype(BF)
    upper = weight.astype(BF)
    lower = (weight - upper.astype(F32)).astype(BF)
    shape = (experts[0], place_ref.shape[1])
    row_index = lax.broadcasted_iota(jnp.int32, shape, 0)
    wanted = (place_ref[...] ^ turn_ref[0]) * experts[1] + experts[2]
    pick = jnp.where(row_index == wanted, 1.0, 0.0).astype(BF)
    chosen = dot32(ranks, pick) == rank_ref[...]
    out_ref[0] = jnp.where(chosen, dot32(upper, pick), 0.0).astype(BF)
    out_ref[1] = jnp.where(chosen, dot32(lower, pick), 0.0).astype(BF)


def combine_body(count, weights_ref, *refs):
    back_ref = refs[-1]
    rows = back_ref.shape[0] // count
    for p in range(count):
        back_ref[p * rows : (p + 1) * rows] = refs[p][...]
    back = back_ref[...]
    total = dot32(weights_ref[0], back) + dot32(weights_ref[1], back)
    for ref in refs[count:-2]:
        total = total + ref[...].astype(F32)
    refs[-2][...] = total.astype(refs[-2].dtype)


def layer(
    queries,
    keys,
    values,
    sinks,
    residual,
    out_weight,
    norm_gain,
    shared_gate,
    shared_up,
    shared_down,
    expert_ids,
    route_weights,
    expert_gate,
    expert_up,
    expert_down,
):
    block_rows, query_width = queries.shape
    ways = lax.axis_size("tp")
    splits = lax.axis_size("sp")
    width_index = lax.axis_index("tp")
    sp_index = lax.axis_index("sp")
    model_width = out_weight.shape[1]
    own = block_rows // ways
    halves = ways // 2
    experts_here = expert_gate.shape[0]
    experts_all = experts_here * splits
    capacity = max(2, 2 * own * TOPK // experts_all)
    slots = splits * capacity

    def over(x, mask):
        return lax.ppermute(x, "tp", [(i, i ^ mask) for i in range(ways)])

    def exchange(x):
        return lax.all_to_all(x, "sp", 0, 0, tiled=True)

    def turned(pieces, masks):
        done = []
        for piece, m in zip(pieces, masks):
            pairs = [(i, i ^ m) for i in range(splits)]
            done.append(lax.ppermute(piece, "sp", pairs) if m else piece)
        return done

    def returned(keep, send, name, first):
        if not turning:
            summed = plus(keep, over(send, 2))
            return [exchange(summed)]
        half = splits // 2
        rows = half * capacity
        pieces = [None] * splits
        for part in (1, 0):
            start = rows * (part ^ first)
            mine = lax.dynamic_slice_in_dim(keep, start, rows, 0)
            other = lax.dynamic_slice_in_dim(send, start, rows, 0)
            other = over(other, 2)
            if part == 0:
                other, summed = lax.optimization_barrier((other, summed))
            summed = plus(mine, other)
            masks = range(part * half, (part + 1) * half)
            for m in masks:
                inner = (m % half) ^ first_low[name]
                pieces[m] = lax.dynamic_slice_in_dim(summed, inner * capacity, capacity, 0)
            pieces[part * half : (part + 1) * half] = turned(
                pieces[part * half : (part + 1) * half], masks
            )
        return pieces

    def plus(a, b):
        return (a.astype(F32) + b.astype(F32)).astype(BF)

    up = [(i, i + 1) for i in range(splits - 1)]
    down = [(i + 1, i) for i in range(splits - 1)]
    keys_t, values_t = keys.T, values.T
    tail = jnp.concatenate([keys_t[:, -WINDOW:], values_t[:, -WINDOW:]], axis=0)
    head = jnp.concatenate([keys_t[:, :WINDOW], values_t[:, :WINDOW]], axis=0)
    before = lax.ppermute(tail, "sp", up)
    after = lax.ppermute(head, "sp", down)
    quarter = HEAD_DIM // 4
    spectrum = ROPE_BASE ** (-np.arange(quarter, dtype=np.float64) / quarter)
    spectrum = np.concatenate([spectrum, spectrum])[:, None].astype(np.float32)
    attended = call(
        functools.partial(attention_body, total_rows=splits * block_rows),
        [((block_rows, query_width), BF)],
        (queries.T, keys_t, values_t, before, after, jnp.asarray(spectrum)),
        scalars=(sp_index.reshape(1), sinks),
        scratch=[
            pltpu.VMEM((block_rows + 2 * WINDOW, HEAD_DIM), BF),
            pltpu.VMEM((HEAD_DIM, block_rows + 2 * WINDOW), BF),
        ],
        flops=12 * block_rows * WINDOW * query_width,
        moved=4 * block_rows * query_width,
    )[0]

    order = width_index ^ jnp.arange(ways, dtype=jnp.int32)
    gain = norm_gain.reshape(1, model_width)
    ids_t = expert_ids.T.reshape(TOPK, ways, own).transpose(1, 0, 2)
    experts = (experts_all, experts_here)
    place = np.arange(slots, dtype=np.int32) // capacity
    rank = (np.arange(slots) % capacity).astype(np.float32)
    turning = splits <= 8
    turn = (sp_index if turning else sp_index * 0).reshape(1)
    combine_weights = []
    for c in range(experts_here):
        combine_weights += call(
            functools.partial(prepare_body, experts=(*experts, c)),
            [((2, own, slots), BF)],
            (expert_ids, route_weights, jnp.asarray(place[None, :]), jnp.asarray(rank[None, :])),
            scalars=(order, turn),
            own=((0, own, 0),),
            flops=4 * own * experts_all * slots,
            moved=4 * own * slots,
        )
    parts = lax.all_gather(attended, "tp", axis=0, tiled=False)
    mixed, outgoing = call(
        functools.partial(dispatch_body, experts=experts),
        [((own, model_width), BF), ((slots, model_width), BF)],
        (
            parts,
            residual,
            out_weight,
            gain,
            ids_t,
            jnp.asarray(place[:, None]),
            jnp.asarray(rank[:, None]),
        ),
        scalars=(order,),
        own=((1, own, 0),),
        flops=2 * own * model_width * (out_weight.shape[0] + slots),
        moved=2 * out_weight.size,
    )
    near = exchange(outgoing)

    outgoing = call(
        functools.partial(second_body, experts=experts),
        [((halves * capacity, model_width), BF)] * (splits * (experts_here - 1)),
        (
            parts,
            residual,
            residual,
            out_weight,
            gain,
            ids_t,
            jnp.asarray(place[:, None]),
            jnp.asarray(rank[:, None]),
        ),
        scalars=(order, turn),
        own=((1, own, 0), (2, own, 2)),
        flops=2 * halves * own * model_width * (out_weight.shape[0] + slots),
        moved=2 * out_weight.size,
    )
    keep, send = call(
        shared_body,
        [((halves, own, model_width), BF)] * 2,
        (parts, residual, out_weight, gain, shared_gate, shared_up, shared_down),
        scalars=(order,),
        scratch=[pltpu.VMEM((block_rows, model_width), BF)],
        flops=2 * block_rows * model_width * (out_weight.shape[0] + 3 * shared_gate.shape[1]),
        moved=2 * out_weight.size,
    )
    got = over(send, 1)
    shared_own = plus(keep[0], got[0])
    shared_far = over(plus(keep[1], got[1]), 2)

    weights = (expert_gate, expert_up, expert_down)
    far = over(near, 2)
    near_pair = over(near, 1)
    far_pair = over(far, 1)
    out_pair, out_near = expert_rows(0, [near_pair, near], *weights)
    from_pair = over(out_pair, 1)
    out_far_pair, out_far = expert_rows(0, [far_pair, far], *weights)
    far_sum = plus(out_far, over(out_far_pair, 1))
    near_sum = plus(out_near, from_pair)
    half = splits // 2
    first_low = {"near": sp_index % half, "mine": 0}
    back = [returned(near_sum, far_sum, "near", sp_index // half)]

    for c in range(1, experts_here):
        pieces = outgoing[splits * (c - 1) : splits * c]
        if turning:
            arrived = turned(pieces, range(splits))
            mine, far = joined(arrived, halves)
        else:
            arrived = exchange(jnp.concatenate(pieces, axis=0))
            arrived = arrived.reshape(splits, halves, capacity, model_width)
            mine, far = (arrived[:, h].reshape(slots, model_width) for h in range(halves))
        far_pair = over(far, 1)
        out_pair, out_far = expert_rows(c, [far_pair, far], *weights)
        far_sum = plus(out_far, over(out_pair, 1))
        pair = over(mine, 1)
        out_pair, out_mine = expert_rows(c, [pair, mine], *weights)
        summed = plus(out_mine, over(out_pair, 1))
        back.append(returned(summed, far_sum, "mine", 0))

    total = None
    for c in range(experts_here):
        last = c == experts_here - 1
        added = (mixed, shared_own, shared_far) if total is None else (total,)
        total = call(
            functools.partial(combine_body, len(back[c])),
            [((own, model_width), BF if last else F32)],
            (combine_weights[c], *back[c], *added),
            scratch=[pltpu.VMEM((slots, model_width), BF)],
            flops=4 * own * slots * model_width,
            moved=2 * slots * model_width,
        )[0]
    return total


def solution(mesh):
    placed = (
        P("sp", "tp"),
        P("sp", "tp"),
        P("sp", "tp"),
        P("tp"),
        P("sp", None),
        P(),
        P(),
        P(None, "tp"),
        P(None, "tp"),
        P("tp", None),
        P("sp", None),
        P(("sp", "tp"), None),
        P("sp", None, "tp"),
        P("sp", None, "tp"),
        P("sp", "tp", None),
    )
    return jax.shard_map(
        layer, mesh=mesh, in_specs=placed, out_specs=P(("sp", "tp"), None), check_vma=False
    )
```

profile of v0, /device:TPU:0, one launch (start us, length us, event | category | flops | bytes accessed | tf_op | source)
XLA Modules:
  0.0 214.5 jit_solution(14893586286576117441)
XLA Ops:
  0.8 4.9 %collective-permute-start = (bf16[128,128]{1,0:T(8,128)(2,1)S(1)}, bf16[128,128]{1,0:T(8,128)(2,1)S(1)}, u32[]{:S(2)}, u32[]{:S(2)}) collective-permute-start(bf16[128,128]{1,0:T(8,128)(2,1)S(1)} %pad_maximum_fusion), channel_id=1, source_target_pairs={{0,4},{4,8},{8,12},{12,16},{16,20},{20,24},{24,28},{1,5},{5,9},{9,... | collective-permute-start | bytes 98312 | tf_op jit(solution)/shard_map/ppermute | solution.py:431
  8.9 2.6 %collective-permute-done.1.after_ref = bf16[128,128]{1,0:T(8,128)(2,1)S(1)} collective-permute-done((bf16[128,128]{1,0:T(8,128)(2,1)S(1)}, bf16[128,128]{1,0:T(8,128)(2,1)S(1)}, u32[]{:S(2)}, u32[]{:S(2)}) %collective-permute-start.1) | collective-permute-done | bytes 32800 | tf_op jit(solution)/shard_map/ppermute | solution.py:432
  12.1 4.3 %shard_map.227 = bf16[384,192]{1,0:T(8,128)(2,1)} custom-call(s32[1]{0:T(128)} %bitcast.turn_ref.first_ref, f32[3]{0:T(128)} %sink_ref.1, bf16[192,384]{1,0:T(8,128)(2,1)} %bitcast.23, bf16[64,384]{1,0:T(8,128)(2,1)} %bitcast.25, bf16[64,384]{1,0:T(8,128)(2,1)} %bitcast.27, bf16[128,128]{1,0:T(8,128)(2,1)} %copy-done.31, bf16[128,128]{1,0:T(8,128)(2,1)} %copy-done.32, ...), custom_call_target="tpu_custom_call" | custom-call | flops 113246208 | bytes 294912 | tf_op jit(solution)/shard_map/pallas_call | solution.py:42
  16.4 9.3 %all-gather = bf16[1536,192]{1,0:T(8,128)(2,1)} all-gather(bf16[384,192]{1,0:T(8,128)(2,1)} %shard_map.227), channel_id=2, replica_groups=mesh['sp'=8,'tp'=4] {'tp'}, dimensions={0}, use_global_device_ids=true | all-gather | bytes 737280 | tf_op jit(solution)/shard_map/all_gather | solution.py:468
  25.6 5.9 %shard_map.228 = (bf16[48,2048]{1,0:T(8,128)(2,1)}, bf16[48,2048]{1,0:T(8,128)(2,1)}, bf16[48,2048]{1,0:T(8,128)(2,1)}, bf16[48,2048]{1,0:T(8,128)(2,1)}, bf16[4...) custom-call(s32[4]{0:T(128)} %iota_xor_fusion.order_ref, ...), custom_call_target="tpu_custom_call" | custom-call | flops 754974720 | bytes 3145728 | tf_op jit(solution)/shard_map/pallas_call | solution.py:42
  31.6 2.5 %collective-permute-start.2 = (bf16[48,2048]{1,0:T(8,128)(2,1)}, bf16[48,2048]{1,0:T(8,128)(2,1)S(1)}, u32[]{:S(2)}, u32[]{:S(2)}) collective-permute-start(bf16[48,2048]{1,0:T(8,128)(2,1)} %get-tuple-element.30), channel_id=1, source_target_pairs={{0,4},{4,0},{8,12},{12,8},{16,20},{20,16},{24,28},{28,24},{1,5},{5... | collective-permute-start | bytes 589832 | tf_op jit(solution)/shard_map/ppermute | solution.py:396
  35.6 2.5 %collective-permute-start.5 = (bf16[48,2048]{1,0:T(8,128)(2,1)}, bf16[48,2048]{1,0:T(8,128)(2,1)S(1)}, u32[]{:S(2)}, u32[]{:S(2)}) collective-permute-start(bf16[48,2048]{1,0:T(8,128)(2,1)} %get-tuple-element.33), channel_id=1, source_target_pairs={{0,16},{4,20},{8,24},{12,28},{16,0},{20,4},{24,8},{28,12},{1,17},{... | collective-permute-start | bytes 589832 | tf_op jit(solution)/shard_map/ppermute | solution.py:396
  39.9 2.7 %collective-permute-start.7 = (bf16[48,2048]{1,0:T(8,128)(2,1)}, bf16[48,2048]{1,0:T(8,128)(2,1)S(1)}, u32[]{:S(2)}, u32[]{:S(2)}) collective-permute-start(bf16[48,2048]{1,0:T(8,128)(2,1)} %get-tuple-element.35), channel_id=1, source_target_pairs={{0,24},{4,28},{8,16},{12,20},{16,8},{20,12},{24,0},{28,4},{1,25},{... | collective-permute-start | bytes 589832 | tf_op jit(solution)/shard_map/ppermute | solution.py:396
  42.5 7.4 %collective-permute-done.3.refs_2_ = bf16[48,2048]{1,0:T(8,128)(2,1)S(1)} collective-permute-done((bf16[48,2048]{1,0:T(8,128)(2,1)}, bf16[48,2048]{1,0:T(8,128)(2,1)S(1)}, u32[]{:S(2)}, u32[]{:S(2)}) %collective-permute-start.3) | collective-permute-done | bytes 196640 | tf_op jit(solution)/shard_map/ppermute | solution.py:396
  52.1 14.8 %collective-permute-done.6.refs_5_ = bf16[48,2048]{1,0:T(8,128)(2,1)S(1)} collective-permute-done((bf16[48,2048]{1,0:T(8,128)(2,1)}, bf16[48,2048]{1,0:T(8,128)(2,1)S(1)}, u32[]{:S(2)}, u32[]{:S(2)}) %collective-permute-start.6) | collective-permute-done | bytes 196640 | tf_op jit(solution)/shard_map/ppermute | solution.py:396
  67.7 2.7 %shard_map.229 = (bf16[192,2048]{1,0:T(8,128)(2,1)}, bf16[192,2048]{1,0:T(8,128)(2,1)}) custom-call(bf16[48,2048]{1,0:T(8,128)(2,1)} %get-tuple-element.29.refs_0_, bf16[48,2048]{1,0:T(8,128)(2,1)} %copy-done.10, bf16[48,2048]{1,0:T(8,128)(2,1)} %copy-done.11, bf16[48,2048]{1,0:T(8,128)(2,1)} %copy-done.12, bf16[48,2048]{1,0:T(8,128)(2,1)} %copy-done.13, ...), custom_call_target="tpu_custom_call" | custom-call | flops 786432 | bytes 3145728 | tf_op jit(solution)/shard_map/pallas_call | solution.py:42
  70.5 7.8 %shard_map.236 = (bf16[2,96,2048]{2,1,0:T(8,128)(2,1)}, bf16[2,96,2048]{2,1,0:T(8,128)(2,1)}) custom-call(s32[4]{0:T(128)} %iota_xor_fusion.order_ref, bf16[4,384,192]{2,1,0:T(8,128)(2,1)} %bitcast.17, bf16[384,2048]{1,0:T(8,128)(2,1)} %residual_ref.3, bf16[768,2048]{1,0:T(8,128)(2,1)} %weight_ref.5, f32[1,2048]{1,0:T(1,128)} %bitcast.29, ...), custom_call_target="tpu_custom_call" | custom-call | flops 1811939328 | bytes 3145728 | tf_op jit(solution)/shard_map/pallas_call | solution.py:42
  78.8 5.0 %shard_map.233 = (bf16[96,2048]{1,0:T(8,128)(2,1)}, bf16[192,2048]{1,0:T(8,128)(2,1)}) custom-call(s32[4]{0:T(128)} %iota_xor_fusion.order_ref, bf16[4,384,192]{2,1,0:T(8,128)(2,1)} %bitcast.18, bf16[384,2048]{1,0:T(8,128)(2,1)} %residual_ref.3, bf16[768,2048]{1,0:T(8,128)(2,1)} %weight_ref.5, f32[1,2048]{1,0:T(1,128)} %bitcast.30, s32[4,2,96]{2,1,0:T(2,128)} %bitcast.32, ...), custom_call_target="tpu_custom_call" | custom-call | flops 377487360 | bytes 3145728 | tf_op jit(solution)/shard_map/pallas_call | solution.py:42
  83.8 9.8 %all-to-all-start = ((bf16[8,24,2048]{2,1,0:T(8,128)(2,1)}), bf16[8,24,2048]{2,1,0:T(8,128)(2,1)S(1)}, u32[]{:S(2)}, u32[]{:S(2)}) async-start(bf16[8,24,2048]{2,1,0:T(8,128)(2,1)} %bitcast.22), calls=%async_computation | async-start | bytes 1572864 | tf_op jit(solution)/shard_map/all_to_all | solution.py:390
  94.7 4.8 %shard_map.231 = (bf16[192,2048]{1,0:T(8,128)(2,1)}, bf16[192,2048]{1,0:T(8,128)(2,1)}) custom-call(bf16[192,2048]{1,0:T(8,128)(2,1)} %copy-done.9, bf16[192,2048]{1,0:T(8,128)(2,1)} %get-tuple-element.40.refs_1_, bf16[2,2048,256]{2,1,0:T(8,128)(2,1)} %refs_2_.7, bf16[2,2048,256]{2,1,0:T(8,128)(2,1)} %refs_3_.7, bf16[2,256,2048]{2,1,0:T(8,128)(2,1)} %refs_4_.7), custom_call_target="tpu_custom_call" | custom-call | flops 1207959552 | bytes 6291456 | tf_op jit(solution)/shard_map/pallas_call | solution.py:272
  101.6 4.8 %shard_map.230 = (bf16[192,2048]{1,0:T(8,128)(2,1)}, bf16[192,2048]{1,0:T(8,128)(2,1)}) custom-call(bf16[192,2048]{1,0:T(8,128)(2,1)} %collective-permute-done.9.refs_0_, bf16[192,2048]{1,0:T(8,128)(2,1)} %get-tuple-element.37.refs_1_, bf16[2,2048,256]{2,1,0:T(8,128)(2,1)} %refs_2_.7, bf16[2,2048,256]{2,1,0:T(8,128)(2,1)} %refs_3_.7, ...), custom_call_target="tpu_custom_call" | custom-call | flops 1207959552 | bytes 6291456 | tf_op jit(solution)/shard_map/pallas_call | solution.py:272
  106.5 7.5 %all-to-all-done = bf16[8,24,2048]{2,1,0:T(8,128)(2,1)S(1)} async-done(((bf16[8,24,2048]{2,1,0:T(8,128)(2,1)}), bf16[8,24,2048]{2,1,0:T(8,128)(2,1)S(1)}, u32[]{:S(2)}, u32[]{:S(2)}) %all-to-all-start) | async-done | bytes 786464 | tf_op jit(solution)/shard_map/all_to_all | solution.py:390
  117.0 17.4 %collective-permute-done.24.refs_1_ = bf16[192,2048]{1,0:T(8,128)(2,1)S(1)} collective-permute-done((bf16[192,2048]{1,0:T(8,128)(2,1)S(1)}, bf16[192,2048]{1,0:T(8,128)(2,1)S(1)}, u32[]{:S(2)}, u32[]{:S(2)}) %collective-permute-start.24) | collective-permute-done | bytes 786464 | tf_op jit(solution)/shard_map/ppermute | solution.py:387
  135.7 4.8 %shard_map.234 = (bf16[192,2048]{1,0:T(8,128)(2,1)}, bf16[192,2048]{1,0:T(8,128)(2,1)}) custom-call(bf16[192,2048]{1,0:T(8,128)(2,1)} %copy-done.7, bf16[192,2048]{1,0:T(8,128)(2,1)} %bitcast.21, bf16[2,2048,256]{2,1,0:T(8,128)(2,1)} %refs_2_.7, bf16[2,2048,256]{2,1,0:T(8,128)(2,1)} %refs_3_.7, bf16[2,256,2048]{2,1,0:T(8,128)(2,1)} %refs_4_.7), custom_call_target="tpu_custom_call" | custom-call | flops 1207959552 | bytes 6291456 | tf_op jit(solution)/shard_map/pallas_call | solution.py:272
  143.0 6.0 %collective-permute-done.13 = bf16[96,2048]{1,0:T(8,128)(2,1)S(1)} collective-permute-done((bf16[96,2048]{1,0:T(8,128)(2,1)S(1)}, bf16[96,2048]{1,0:T(8,128)(2,1)S(1)}, u32[]{:S(2)}, u32[]{:S(2)}) %collective-permute-start.13) | collective-permute-done | bytes 393248 | tf_op jit(solution)/shard_map/ppermute | solution.py:387
  149.9 4.8 %shard_map.235 = (bf16[192,2048]{1,0:T(8,128)(2,1)}, bf16[192,2048]{1,0:T(8,128)(2,1)}) custom-call(bf16[192,2048]{1,0:T(8,128)(2,1)} %copy-done.8, bf16[192,2048]{1,0:T(8,128)(2,1)} %copy-done.6, bf16[2,2048,256]{2,1,0:T(8,128)(2,1)} %refs_2_.7, bf16[2,2048,256]{2,1,0:T(8,128)(2,1)} %refs_3_.7, bf16[2,256,2048]{2,1,0:T(8,128)(2,1)} %refs_4_.7), custom_call_target="tpu_custom_call" | custom-call | flops 1207959552 | bytes 6291456 | tf_op jit(solution)/shard_map/pallas_call | solution.py:272
  160.2 9.6 %collective-permute-done.28 = bf16[96,2048]{1,0:T(8,128)(2,1)S(1)} collective-permute-done((bf16[96,2048]{1,0:T(8,128)(2,1)S(1)}, bf16[96,2048]{1,0:T(8,128)(2,1)S(1)}, u32[]{:S(2)}, u32[]{:S(2)}) %collective-permute-start.28) | collective-permute-done | bytes 393248 | tf_op jit(solution)/shard_map/ppermute | solution.py:387
  170.0 3.0 %collective-permute-start.32 = (bf16[24,2048]{1,0:T(8,128)(2,1)S(1)}, bf16[24,2048]{1,0:T(8,128)(2,1)S(1)}, u32[]{:S(2)}, u32[]{:S(2)}) collective-permute-start(bf16[24,2048]{1,0:T(8,128)(2,1)S(1)} %get-tuple-element.62), channel_id=1, source_target_pairs={{0,16},{4,20},{8,24},{12,28},{16,0},{20,4},{24,8},{28,12},{1,17},{... | collective-permute-start | bytes 294920 | tf_op jit(solution)/shard_map/ppermute | solution.py:396
  173.0 4.5 %collective-permute-done.27 = bf16[96,2048]{1,0:T(8,128)(2,1)S(1)} collective-permute-done((bf16[96,2048]{1,0:T(8,128)(2,1)S(1)}, bf16[96,2048]{1,0:T(8,128)(2,1)S(1)}, u32[]{:S(2)}, u32[]{:S(2)}) %collective-permute-start.27) | collective-permute-done | bytes 393248 | tf_op jit(solution)/shard_map/ppermute | solution.py:387
  182.1 3.5 %collective-permute-start.35 = (bf16[24,2048]{1,0:T(8,128)(2,1)S(1)}, bf16[24,2048]{1,0:T(8,128)(2,1)S(1)}, u32[]{:S(2)}, u32[]{:S(2)}) collective-permute-start(bf16[24,2048]{1,0:T(8,128)(2,1)S(1)} %get-tuple-element.59), channel_id=1, source_target_pairs={{0,28},{4,24},{8,20},{12,16},{16,12},{20,8},{24,4},{28,0},{1,29},{... | collective-permute-start | bytes 294920 | tf_op jit(solution)/shard_map/ppermute | solution.py:396
  186.0 4.7 %collective-permute-done.33.refs_5_ = bf16[24,2048]{1,0:T(8,128)(2,1)S(1)} collective-permute-done((bf16[24,2048]{1,0:T(8,128)(2,1)S(1)}, bf16[24,2048]{1,0:T(8,128)(2,1)S(1)}, u32[]{:S(2)}, u32[]{:S(2)}) %collective-permute-start.33) | collective-permute-done | bytes 98336 | tf_op jit(solution)/shard_map/ppermute | solution.py:396
  190.7 3.0 %collective-permute-start.17 = (bf16[24,2048]{1,0:T(8,128)(2,1)S(1)}, bf16[24,2048]{1,0:T(8,128)(2,1)S(1)}, u32[]{:S(2)}, u32[]{:S(2)}) collective-permute-start(bf16[24,2048]{1,0:T(8,128)(2,1)S(1)} %get-tuple-element.71), channel_id=1, source_target_pairs={{0,12},{4,8},{8,4},{12,0},{16,28},{20,24},{24,20},{28,16},{1,13},{... | collective-permute-start | bytes 294920 | tf_op jit(solution)/shard_map/ppermute | solution.py:396
  196.9 2.6 %collective-permute-start.20 = (bf16[24,2048]{1,0:T(8,128)(2,1)S(1)}, bf16[24,2048]{1,0:T(8,128)(2,1)S(1)}, u32[]{:S(2)}, u32[]{:S(2)}) collective-permute-start(bf16[24,2048]{1,0:T(8,128)(2,1)S(1)} %get-tuple-element.68), channel_id=1, source_target_pairs={{0,24},{4,28},{8,16},{12,20},{16,8},{20,12},{24,0},{28,4},{1,25},{... | collective-permute-start | bytes 294920 | tf_op jit(solution)/shard_map/ppermute | solution.py:396
  202.9 2.6 %shard_map.232.weights_ref = bf16[2,96,192]{2,1,0:T(8,128)(2,1)} custom-call(s32[4]{0:T(128)} %iota_xor_fusion.order_ref, s32[1]{0:T(128)} %bitcast.turn_ref.first_ref, s32[384,2]{1,0:T(8,128)} %copy.29.ids_ref, f32[96,2]{1,0:T(8,128)} %copy.30.route_ref, s32[1,192]{1,0:T(1,128)} %constant.56.clone.place_ref, f32[1,192]{1,0:T(1,128)} %constant.57.clone.rank_ref), custom_call_target="tpu_custom_call" | custom-call | flops 1179648 | bytes 73728 | tf_op jit(solution)/shard_map/pallas_call | solution.py:42
  205.5 2.5 %shard_map.226.weights_ref = bf16[2,96,192]{2,1,0:T(8,128)(2,1)} custom-call(s32[4]{0:T(128)} %iota_xor_fusion.order_ref, s32[1]{0:T(128)} %bitcast.turn_ref.first_ref, s32[384,2]{1,0:T(8,128)} %copy.29.ids_ref, f32[96,2]{1,0:T(8,128)} %copy.30.route_ref, s32[1,192]{1,0:T(1,128)} %constant.56.clone.place_ref, f32[1,192]{1,0:T(1,128)} %constant.57.clone.rank_ref), custom_call_target="tpu_custom_call" | custom-call | flops 1179648 | bytes 73728 | tf_op jit(solution)/shard_map/pallas_call | solution.py:42
  208.1 2.9 %shard_map.237.refs_8_ = f32[96,2048]{1,0:T(8,128)} custom-call(bf16[2,96,192]{2,1,0:T(8,128)(2,1)} %shard_map.232.weights_ref, bf16[24,2048]{1,0:T(8,128)(2,1)} %get-tuple-element.66.refs_0_, bf16[24,2048]{1,0:T(8,128)(2,1)} %copy-done.23, bf16[24,2048]{1,0:T(8,128)(2,1)} %copy-done.25, bf16[24,2048]{1,0:T(8,128)(2,1)} %copy-done.27, ...), custom_call_target="tpu_custom_call" | custom-call | flops 150994944 | bytes 786432 | tf_op jit(solution)/shard_map/pallas_call | solution.py:42
  211.8 2.6 %shard_map.238 = bf16[96,2048]{1,0:T(8,128)(2,1)} custom-call(bf16[2,96,192]{2,1,0:T(8,128)(2,1)} %shard_map.226.weights_ref, bf16[24,2048]{1,0:T(8,128)(2,1)} %get-tuple-element.74.refs_0_, bf16[24,2048]{1,0:T(8,128)(2,1)} %copy-done.17, bf16[24,2048]{1,0:T(8,128)(2,1)} %copy-done.18, bf16[24,2048]{1,0:T(8,128)(2,1)} %copy-done.24, ...), custom_call_target="tpu_custom_call" | custom-call | flops 150994944 | bytes 786432 | tf_op jit(solution)/shard_map/pallas_call | solution.py:42
  (153 shorter events, 40.0 us)
Async XLA Ops:
  34.0 15.9 %collective-permute-start.3 = (bf16[48,2048]{1,0:T(8,128)(2,1)}, bf16[48,2048]{1,0:T(8,128)(2,1)S(1)}, u32[]{:S(2)}, u32[]{:S(2)}) collective-permute-start(bf16[48,2048]{1,0:T(8,128)(2,1)} %get-tuple-element.31), channel_id=1, source_target_pairs={{0,8},{4,12},{8,0},{12,4},{16,24},{20,28},{24,16},{28,20},{1,9},{5... | collective-permute-start | bytes 589832 | tf_op jit(solution)/shard_map/ppermute | solution.py:396
  35.6 16.5 %collective-permute-start.4 = (bf16[48,2048]{1,0:T(8,128)(2,1)}, bf16[48,2048]{1,0:T(8,128)(2,1)S(1)}, u32[]{:S(2)}, u32[]{:S(2)}) collective-permute-start(bf16[48,2048]{1,0:T(8,128)(2,1)} %get-tuple-element.32), channel_id=1, source_target_pairs={{0,12},{4,8},{8,4},{12,0},{16,28},{20,24},{24,20},{28,16},{1,13},{... | collective-permute-start | bytes 589832 | tf_op jit(solution)/shard_map/ppermute | solution.py:396
  35.6 16.5 %collective-permute-start.5 = (bf16[48,2048]{1,0:T(8,128)(2,1)}, bf16[48,2048]{1,0:T(8,128)(2,1)S(1)}, u32[]{:S(2)}, u32[]{:S(2)}) collective-permute-start(bf16[48,2048]{1,0:T(8,128)(2,1)} %get-tuple-element.33), channel_id=1, source_target_pairs={{0,16},{4,20},{8,24},{12,28},{16,0},{20,4},{24,8},{28,12},{1,17},{... | collective-permute-start | bytes 589832 | tf_op jit(solution)/shard_map/ppermute | solution.py:396
  38.1 28.8 %collective-permute-start.6 = (bf16[48,2048]{1,0:T(8,128)(2,1)}, bf16[48,2048]{1,0:T(8,128)(2,1)S(1)}, u32[]{:S(2)}, u32[]{:S(2)}) collective-permute-start(bf16[48,2048]{1,0:T(8,128)(2,1)} %get-tuple-element.34), channel_id=1, source_target_pairs={{0,20},{4,16},{8,28},{12,24},{16,4},{20,0},{24,12},{28,8},{1,21},{... | collective-permute-start | bytes 589832 | tf_op jit(solution)/shard_map/ppermute | solution.py:396
  39.9 27.0 %collective-permute-start.7 = (bf16[48,2048]{1,0:T(8,128)(2,1)}, bf16[48,2048]{1,0:T(8,128)(2,1)S(1)}, u32[]{:S(2)}, u32[]{:S(2)}) collective-permute-start(bf16[48,2048]{1,0:T(8,128)(2,1)} %get-tuple-element.35), channel_id=1, source_target_pairs={{0,24},{4,28},{8,16},{12,20},{16,8},{20,12},{24,0},{28,4},{1,25},{... | collective-permute-start | bytes 589832 | tf_op jit(solution)/shard_map/ppermute | solution.py:396
  49.9 17.0 %collective-permute-start.8 = (bf16[48,2048]{1,0:T(8,128)(2,1)}, bf16[48,2048]{1,0:T(8,128)(2,1)S(1)}, u32[]{:S(2)}, u32[]{:S(2)}) collective-permute-start(bf16[48,2048]{1,0:T(8,128)(2,1)} %get-tuple-element.36), channel_id=1, source_target_pairs={{0,28},{4,24},{8,20},{12,16},{16,12},{20,8},{24,4},{28,0},{1,29},{... | collective-permute-start | bytes 589832 | tf_op jit(solution)/shard_map/ppermute | solution.py:396
  70.5 23.3 %collective-permute-start.11 = (bf16[192,2048]{1,0:T(8,128)(2,1)}, bf16[192,2048]{1,0:T(8,128)(2,1)S(1)}, u32[]{:S(2)}, u32[]{:S(2)}) collective-permute-start(bf16[192,2048]{1,0:T(8,128)(2,1)} %get-tuple-element.40.refs_1_), channel_id=1, source_target_pairs={{0,1},{1,0},{2,3},{3,2},{4,5},{5,4},{6,7},{7,6},{8,9},{9,8},{10,11... | collective-permute-start | bytes 2359304 | tf_op jit(solution)/shard_map/ppermute | solution.py:387
  78.3 21.8 %collective-permute-start.36 = (bf16[2,96,2048]{2,1,0:T(8,128)(2,1)}, bf16[2,96,2048]{2,1,0:T(8,128)(2,1)S(1)}, u32[]{:S(2)}, u32[]{:S(2)}) collective-permute-start(bf16[2,96,2048]{2,1,0:T(8,128)(2,1)} %get-tuple-element.52), channel_id=1, source_target_pairs={{0,1},{1,0},{2,3},{3,2},{4,5},{5,4},{6,7},{7,6},{8,9},{9,8},{10,11... | collective-permute-start | bytes 2359304 | tf_op jit(solution)/shard_map/ppermute | solution.py:387
  83.8 30.2 %all-to-all-start = ((bf16[8,24,2048]{2,1,0:T(8,128)(2,1)}), bf16[8,24,2048]{2,1,0:T(8,128)(2,1)S(1)}, u32[]{:S(2)}, u32[]{:S(2)}) async-start(bf16[8,24,2048]{2,1,0:T(8,128)(2,1)} %bitcast.22), calls=%async_computation | async-start | bytes 1572864 | tf_op jit(solution)/shard_map/all_to_all | solution.py:390
  99.5 15.1 %collective-permute-start.12 = (bf16[192,2048]{1,0:T(8,128)(2,1)}, bf16[192,2048]{1,0:T(8,128)(2,1)S(1)}, u32[]{:S(2)}, u32[]{:S(2)}) collective-permute-start(bf16[192,2048]{1,0:T(8,128)(2,1)} %get-tuple-element.42), channel_id=1, source_target_pairs={{0,1},{1,0},{2,3},{3,2},{4,5},{5,4},{6,7},{7,6},{8,9},{9,8},{10,11... | collective-permute-start | bytes 2359304 | tf_op jit(solution)/shard_map/ppermute | solution.py:387
  101.1 79.5 %collective-permute-start.37 = (bf16[96,2048]{1,0:T(8,128)(2,1)S(1)}, bf16[96,2048]{1,0:T(8,128)(2,1)}, u32[]{:S(2)}, u32[]{:S(2)}) collective-permute-start(bf16[96,2048]{1,0:T(8,128)(2,1)S(1)} %get-tuple-element.53), channel_id=1, source_target_pairs={{0,2},{1,3},{2,0},{3,1},{4,6},{5,7},{6,4},{7,5},{8,10},{9,11},{10,... | collective-permute-start | bytes 1179656 | tf_op jit(solution)/shard_map/ppermute | solution.py:387
  106.5 10.1 %collective-permute-start.10 = (bf16[192,2048]{1,0:T(8,128)(2,1)}, bf16[192,2048]{1,0:T(8,128)(2,1)S(1)}, u32[]{:S(2)}, u32[]{:S(2)}) collective-permute-start(bf16[192,2048]{1,0:T(8,128)(2,1)} %get-tuple-element.39), channel_id=1, source_target_pairs={{0,1},{1,0},{2,3},{3,2},{4,5},{5,4},{6,7},{7,6},{8,9},{9,8},{10,11... | collective-permute-start | bytes 2359304 | tf_op jit(solution)/shard_map/ppermute | solution.py:387
  114.1 20.4 %collective-permute-start.24 = (bf16[192,2048]{1,0:T(8,128)(2,1)S(1)}, bf16[192,2048]{1,0:T(8,128)(2,1)S(1)}, u32[]{:S(2)}, u32[]{:S(2)}) collective-permute-start(bf16[192,2048]{1,0:T(8,128)(2,1)S(1)} %bitcast.19), channel_id=1, source_target_pairs={{0,2},{1,3},{2,0},{3,1},{4,6},{5,7},{6,4},{7,5},{8,10},{9,11},{10,... | collective-permute-start | bytes 2359304 | tf_op jit(solution)/shard_map/ppermute | solution.py:387
  114.6 20.2 %collective-permute-start.22 = (bf16[192,2048]{1,0:T(8,128)(2,1)S(1)}, bf16[192,2048]{1,0:T(8,128)(2,1)S(1)}, u32[]{:S(2)}, u32[]{:S(2)}) collective-permute-start(bf16[192,2048]{1,0:T(8,128)(2,1)S(1)} %bitcast.20), channel_id=1, source_target_pairs={{0,1},{1,0},{2,3},{3,2},{4,5},{5,4},{6,7},{7,6},{8,9},{9,8},{10,11... | collective-permute-start | bytes 2359304 | tf_op jit(solution)/shard_map/ppermute | solution.py:387
  115.0 27.9 %collective-permute-start.14 = (bf16[96,2048]{1,0:T(8,128)(2,1)S(1)}, bf16[96,2048]{1,0:T(8,128)(2,1)S(1)}, u32[]{:S(2)}, u32[]{:S(2)}) collective-permute-start(bf16[96,2048]{1,0:T(8,128)(2,1)S(1)} %get-tuple-element.57), channel_id=1, source_target_pairs={{0,2},{1,3},{2,0},{3,1},{4,6},{5,7},{6,4},{7,5},{8,10},{9,11},{10,... | collective-permute-start | bytes 1179656 | tf_op jit(solution)/shard_map/ppermute | solution.py:387
  116.5 32.5 %collective-permute-start.13 = (bf16[96,2048]{1,0:T(8,128)(2,1)S(1)}, bf16[96,2048]{1,0:T(8,128)(2,1)S(1)}, u32[]{:S(2)}, u32[]{:S(2)}) collective-permute-start(bf16[96,2048]{1,0:T(8,128)(2,1)S(1)} %get-tuple-element.58), channel_id=1, source_target_pairs={{0,2},{1,3},{2,0},{3,1},{4,6},{5,7},{6,4},{7,5},{8,10},{9,11},{10,... | collective-permute-start | bytes 1179656 | tf_op jit(solution)/shard_map/ppermute | solution.py:387
  134.5 14.6 %collective-permute-start.25 = (bf16[192,2048]{1,0:T(8,128)(2,1)S(1)}, bf16[192,2048]{1,0:T(8,128)(2,1)S(1)}, u32[]{:S(2)}, u32[]{:S(2)}) collective-permute-start(bf16[192,2048]{1,0:T(8,128)(2,1)S(1)} %collective-permute-done.24.refs_1_), channel_id=1, source_target_pairs={{0,1},{1,0},{2,3},{3,2},{4,5},{5,4},{6,7},{7,6},{8,9},{9,8},{10,11... | collective-permute-start | bytes 2359304 | tf_op jit(solution)/shard_map/ppermute | solution.py:387
  140.5 17.9 %collective-permute-start.23 = (bf16[192,2048]{1,0:T(8,128)(2,1)}, bf16[192,2048]{1,0:T(8,128)(2,1)S(1)}, u32[]{:S(2)}, u32[]{:S(2)}) collective-permute-start(bf16[192,2048]{1,0:T(8,128)(2,1)} %get-tuple-element.46), channel_id=1, source_target_pairs={{0,1},{1,0},{2,3},{3,2},{4,5},{5,4},{6,7},{7,6},{8,9},{9,8},{10,11... | collective-permute-start | bytes 2359304 | tf_op jit(solution)/shard_map/ppermute | solution.py:387
  155.6 26.5 %collective-permute-start.15 = (bf16[24,2048]{1,0:T(8,128)(2,1)S(1)}, bf16[24,2048]{1,0:T(8,128)(2,1)S(1)}, u32[]{:S(2)}, u32[]{:S(2)}) collective-permute-start(bf16[24,2048]{1,0:T(8,128)(2,1)S(1)} %get-tuple-element.73), channel_id=1, source_target_pairs={{0,4},{4,0},{8,12},{12,8},{16,20},{20,16},{24,28},{28,24},{1,5},{5... | collective-permute-start | bytes 294920 | tf_op jit(solution)/shard_map/ppermute | solution.py:396
  157.4 28.2 %collective-permute-start.16 = (bf16[24,2048]{1,0:T(8,128)(2,1)S(1)}, bf16[24,2048]{1,0:T(8,128)(2,1)S(1)}, u32[]{:S(2)}, u32[]{:S(2)}) collective-permute-start(bf16[24,2048]{1,0:T(8,128)(2,1)S(1)} %get-tuple-element.72), channel_id=1, source_target_pairs={{0,8},{4,12},{8,0},{12,4},{16,24},{20,28},{24,16},{28,20},{1,9},{5... | collective-permute-start | bytes 294920 | tf_op jit(solution)/shard_map/ppermute | solution.py:396
  157.8 12.1 %collective-permute-start.28 = (bf16[96,2048]{1,0:T(8,128)(2,1)S(1)}, bf16[96,2048]{1,0:T(8,128)(2,1)S(1)}, u32[]{:S(2)}, u32[]{:S(2)}) collective-permute-start(bf16[96,2048]{1,0:T(8,128)(2,1)S(1)} %get-tuple-element.55), channel_id=1, source_target_pairs={{0,2},{1,3},{2,0},{3,1},{4,6},{5,7},{6,4},{7,5},{8,10},{9,11},{10,... | collective-permute-start | bytes 1179656 | tf_op jit(solution)/shard_map/ppermute | solution.py:387
  158.9 18.7 %collective-permute-start.27 = (bf16[96,2048]{1,0:T(8,128)(2,1)S(1)}, bf16[96,2048]{1,0:T(8,128)(2,1)S(1)}, u32[]{:S(2)}, u32[]{:S(2)}) collective-permute-start(bf16[96,2048]{1,0:T(8,128)(2,1)S(1)} %get-tuple-element.56), channel_id=1, source_target_pairs={{0,2},{1,3},{2,0},{3,1},{4,6},{5,7},{6,4},{7,5},{8,10},{9,11},{10,... | collective-permute-start | bytes 1179656 | tf_op jit(solution)/shard_map/ppermute | solution.py:387
  170.0 15.9 %collective-permute-start.32 = (bf16[24,2048]{1,0:T(8,128)(2,1)S(1)}, bf16[24,2048]{1,0:T(8,128)(2,1)S(1)}, u32[]{:S(2)}, u32[]{:S(2)}) collective-permute-start(bf16[24,2048]{1,0:T(8,128)(2,1)S(1)} %get-tuple-element.62), channel_id=1, source_target_pairs={{0,16},{4,20},{8,24},{12,28},{16,0},{20,4},{24,8},{28,12},{1,17},{... | collective-permute-start | bytes 294920 | tf_op jit(solution)/shard_map/ppermute | solution.py:396
  177.5 13.2 %collective-permute-start.33 = (bf16[24,2048]{1,0:T(8,128)(2,1)S(1)}, bf16[24,2048]{1,0:T(8,128)(2,1)S(1)}, u32[]{:S(2)}, u32[]{:S(2)}) collective-permute-start(bf16[24,2048]{1,0:T(8,128)(2,1)S(1)} %get-tuple-element.61), channel_id=1, source_target_pairs={{0,20},{4,16},{8,28},{12,24},{16,4},{20,0},{24,12},{28,8},{1,21},{... | collective-permute-start | bytes 294920 | tf_op jit(solution)/shard_map/ppermute | solution.py:396
  180.7 10.1 %collective-permute-start.34 = (bf16[24,2048]{1,0:T(8,128)(2,1)S(1)}, bf16[24,2048]{1,0:T(8,128)(2,1)S(1)}, u32[]{:S(2)}, u32[]{:S(2)}) collective-permute-start(bf16[24,2048]{1,0:T(8,128)(2,1)S(1)} %get-tuple-element.60), channel_id=1, source_target_pairs={{0,24},{4,28},{8,16},{12,20},{16,8},{20,12},{24,0},{28,4},{1,25},{... | collective-permute-start | bytes 294920 | tf_op jit(solution)/shard_map/ppermute | solution.py:396
  182.1 11.6 %collective-permute-start.35 = (bf16[24,2048]{1,0:T(8,128)(2,1)S(1)}, bf16[24,2048]{1,0:T(8,128)(2,1)S(1)}, u32[]{:S(2)}, u32[]{:S(2)}) collective-permute-start(bf16[24,2048]{1,0:T(8,128)(2,1)S(1)} %get-tuple-element.59), channel_id=1, source_target_pairs={{0,28},{4,24},{8,20},{12,16},{16,12},{20,8},{24,4},{28,0},{1,29},{... | collective-permute-start | bytes 294920 | tf_op jit(solution)/shard_map/ppermute | solution.py:396
  186.0 10.9 %collective-permute-start.30 = (bf16[24,2048]{1,0:T(8,128)(2,1)S(1)}, bf16[24,2048]{1,0:T(8,128)(2,1)S(1)}, u32[]{:S(2)}, u32[]{:S(2)}) collective-permute-start(bf16[24,2048]{1,0:T(8,128)(2,1)S(1)} %get-tuple-element.64), channel_id=1, source_target_pairs={{0,8},{4,12},{8,0},{12,4},{16,24},{20,28},{24,16},{28,20},{1,9},{5... | collective-permute-start | bytes 294920 | tf_op jit(solution)/shard_map/ppermute | solution.py:396
  190.7 20.3 %collective-permute-start.17 = (bf16[24,2048]{1,0:T(8,128)(2,1)S(1)}, bf16[24,2048]{1,0:T(8,128)(2,1)S(1)}, u32[]{:S(2)}, u32[]{:S(2)}) collective-permute-start(bf16[24,2048]{1,0:T(8,128)(2,1)S(1)} %get-tuple-element.71), channel_id=1, source_target_pairs={{0,12},{4,8},{8,4},{12,0},{16,28},{20,24},{24,20},{28,16},{1,13},{... | collective-permute-start | bytes 294920 | tf_op jit(solution)/shard_map/ppermute | solution.py:396
  193.7 17.3 %collective-permute-start.18 = (bf16[24,2048]{1,0:T(8,128)(2,1)S(1)}, bf16[24,2048]{1,0:T(8,128)(2,1)S(1)}, u32[]{:S(2)}, u32[]{:S(2)}) collective-permute-start(bf16[24,2048]{1,0:T(8,128)(2,1)S(1)} %get-tuple-element.70), channel_id=1, source_target_pairs={{0,16},{4,20},{8,24},{12,28},{16,0},{20,4},{24,8},{28,12},{1,17},{... | collective-permute-start | bytes 294920 | tf_op jit(solution)/shard_map/ppermute | solution.py:396
  195.5 15.5 %collective-permute-start.19 = (bf16[24,2048]{1,0:T(8,128)(2,1)S(1)}, bf16[24,2048]{1,0:T(8,128)(2,1)S(1)}, u32[]{:S(2)}, u32[]{:S(2)}) collective-permute-start(bf16[24,2048]{1,0:T(8,128)(2,1)S(1)} %get-tuple-element.69), channel_id=1, source_target_pairs={{0,20},{4,16},{8,28},{12,24},{16,4},{20,0},{24,12},{28,8},{1,21},{... | collective-permute-start | bytes 294920 | tf_op jit(solution)/shard_map/ppermute | solution.py:396
  196.9 14.2 %collective-permute-start.20 = (bf16[24,2048]{1,0:T(8,128)(2,1)S(1)}, bf16[24,2048]{1,0:T(8,128)(2,1)S(1)}, u32[]{:S(2)}, u32[]{:S(2)}) collective-permute-start(bf16[24,2048]{1,0:T(8,128)(2,1)S(1)} %get-tuple-element.68), channel_id=1, source_target_pairs={{0,24},{4,28},{8,16},{12,20},{16,8},{20,12},{24,0},{28,4},{1,25},{... | collective-permute-start | bytes 294920 | tf_op jit(solution)/shard_map/ppermute | solution.py:396
  199.5 11.6 %collective-permute-start.21 = (bf16[24,2048]{1,0:T(8,128)(2,1)S(1)}, bf16[24,2048]{1,0:T(8,128)(2,1)S(1)}, u32[]{:S(2)}, u32[]{:S(2)}) collective-permute-start(bf16[24,2048]{1,0:T(8,128)(2,1)S(1)} %get-tuple-element.67), channel_id=1, source_target_pairs={{0,28},{4,24},{8,20},{12,16},{16,12},{20,8},{24,4},{28,0},{1,29},{... | collective-permute-start | bytes 294920 | tf_op jit(solution)/shard_map/ppermute | solution.py:396
  (42 other events, 408.4 us)
where the time goes:
time: 215 us; the launch traced here: 214 us
  waiting for transfers between devices  77.9 us (36%)
  starting transfers between devices  57.7 us (27%)
  Pallas kernels  55.6 us (26%)
  local copies, waits for them, and re-layouts  10.3 us (5%)
  blocking collectives  9.27 us (4%)
  other arithmetic  3.06 us (1%)
    ppermute x15, waiting for transfers between devices, over(): return lax.ppermute(x, 'tp', [(i, i ^ mask) for i in range(ways)])  39.5 us
    pallas_call x9, Pallas kernels, call(): pl.pallas_call(body, out_shape=[jax.ShapeDtypeStruct(shape, kind) for sha...  36.4 us
    ppermute x21, starting transfers between devices, turned(): done.append(lax.ppermute(piece, 'sp', pairs) if m else piece)  34.8 us
    ppermute x21, waiting for transfers between devices, turned(): done.append(lax.ppermute(piece, 'sp', pairs) if m else piece)  28.4 us
    pallas_call x4, Pallas kernels, expert_rows(): pl.pallas_call(functools.partial(expert_body, c, count), out_shape=[jax.S...  19.2 us
    all_to_all x1, starting transfers between devices, exchange(): return lax.all_to_all(x, 'sp', 0, 0, tiled=True)  9.85 us
    all_gather x1, blocking collectives, layer(): parts = lax.all_gather(attended, 'tp', axis=0, tiled=False)  9.27 us
    all_to_all x1, waiting for transfers between devices, exchange(): return lax.all_to_all(x, 'sp', 0, 0, tiled=True)  7.52 us
  transfers between devices with their start and end apart: 39, of which 11 were waited for; matrix products, arithmetic and copies ran while one was open for 3% of the time, Pallas kernels for 19%

commit v1 on v0

v1 whole, which is shorter than its diff:
```python
import functools

import jax
import jax.numpy as jnp
import numpy as np
from jax import lax
from jax.experimental import pallas as pl
from jax.experimental.pallas import tpu as pltpu
from jax.sharding import PartitionSpec as P

HEAD_DIM = 64
WINDOW = 128
GRID_W = 64
TOPK = 2
ROPE_BASE = 10000.0
NEG_LARGE = -1e30
NORM_EPSILON = 1e-06

BF = jnp.bfloat16
F32 = jnp.float32
VMEM_LIMIT = 20 * 1024 * 1024


def dot32(a, b):
    return jnp.dot(a, b, preferred_element_type=F32)


def call(body, outs, operands, scalars=(), scratch=(), flops=0, moved=0, final=False):
    local = pl.BlockSpec(memory_space=pltpu.VMEM)
    grid_spec = pltpu.PrefetchScalarGridSpec(
        num_scalar_prefetch=len(scalars),
        grid=(),
        in_specs=[local] * len(operands),
        out_specs=[local] * len(outs),
        scratch_shapes=list(scratch),
    )
    shape_of = jax.ShapeDtypeStruct if final else pltpu.VMEM
    return pl.pallas_call(
        body,
        out_shape=[shape_of(shape, kind) for shape, kind in outs],
        grid_spec=grid_spec,
        compiler_params=pltpu.CompilerParams(vmem_limit_bytes=VMEM_LIMIT),
        cost_estimate=pl.CostEstimate(flops=flops, bytes_accessed=moved, transcendentals=0),
    )(*scalars, *(pltpu.with_memory_space_constraint(x, pltpu.VMEM) for x in operands))


def attention_body(
    tp_ref, first_ref, sink_ref, q_ref, k_ref, v_ref, before_ref, after_ref, spectrum_ref,
    *refs, total_rows,
):
    outs, (out_ref, keys_ref, values_ref) = refs[:-3], refs[-3:]
    key_width, rows = k_ref.shape
    key_heads = key_width // HEAD_DIM
    group = q_ref.shape[0] // key_width
    wide = rows + 2 * WINDOW
    quarter = HEAD_DIM // 4
    first_row = first_ref[0] * rows
    place = lax.broadcasted_iota(jnp.int32, (2 * quarter, wide), 1) + (first_row - WINDOW)
    lane_row = lax.broadcasted_iota(jnp.int32, (2 * quarter, wide), 0)
    shift = GRID_W.bit_length() - 1
    at = jnp.where(
        lane_row < quarter, lax.shift_right_arithmetic(place, shift), place & (GRID_W - 1)
    )
    angles = at.astype(F32) * spectrum_ref[...]
    cosine, sine = jnp.cos(angles), jnp.sin(angles)

    def turn(x, start):
        u = x.astype(F32)
        end = start + x.shape[1]
        pieces = []
        for half in range(2):
            c = cosine[half * quarter : (half + 1) * quarter, start:end]
            s = sine[half * quarter : (half + 1) * quarter, start:end]
            former = u[2 * half * quarter : (2 * half + 1) * quarter]
            latter = u[(2 * half + 1) * quarter : (2 * half + 2) * quarter]
            pieces.append(former * c - latter * s)
            pieces.append(former * s + latter * c)
        return jnp.concatenate(pieces, axis=0)

    query_index = lax.broadcasted_iota(jnp.int32, (3 * WINDOW, WINDOW), 1)
    key_index = lax.broadcasted_iota(jnp.int32, (3 * WINDOW, WINDOW), 0)
    apart = key_index - query_index
    near = (apart >= 0) & (apart <= 2 * WINDOW)
    blocks = rows // WINDOW
    finished = [[] for _ in range(blocks)]
    for g in range(key_heads):
        cut = slice(g * HEAD_DIM, (g + 1) * HEAD_DIM)
        late = slice(key_width + g * HEAD_DIM, key_width + (g + 1) * HEAD_DIM)
        keys = jnp.concatenate([before_ref[cut], k_ref[cut], after_ref[cut]], axis=1)
        keys_ref[...] = turn(keys, 0).T.astype(BF)
        values_ref[...] = jnp.concatenate([before_ref[late], v_ref[cut], after_ref[late]], axis=1)
        turned = [
            turn(q_ref[h * HEAD_DIM : (h + 1) * HEAD_DIM], WINDOW).astype(BF)
            for h in range(g * group, (g + 1) * group)
        ]
        sink = jnp.concatenate(
            [jnp.full((1, WINDOW), sink_ref[h], F32) for h in range(g * group, (g + 1) * group)],
            axis=1,
        )
        for b in range(blocks):
            key_at = key_index + (first_row + (b - 1) * WINDOW)
            allowed = near & (key_at >= 0) & (key_at < total_rows)
            penalty = jnp.where(allowed, 0.0, NEG_LARGE)
            penalty = jnp.concatenate([penalty] * group, axis=1)
            heads = jnp.concatenate(
                [q[:, b * WINDOW : (b + 1) * WINDOW] for q in turned], axis=1
            )
            scores = dot32(keys_ref[b * WINDOW : (b + 3) * WINDOW], heads)
            scores = scores * HEAD_DIM ** (-0.5) + penalty
            highest = jnp.maximum(jnp.max(scores, axis=0, keepdims=True), sink)
            lifted = jnp.exp(scores - highest)
            denominator = jnp.sum(lifted, axis=0, keepdims=True) + jnp.exp(sink - highest)
            probabilities = (lifted * (1.0 / denominator)).astype(BF)
            result = dot32(values_ref[:, b * WINDOW : (b + 3) * WINDOW], probabilities)
            for i in range(group):
                finished[b].append(result[:, i * WINDOW : (i + 1) * WINDOW].T.astype(BF))
    for b in range(blocks):
        out_ref[b * WINDOW : (b + 1) * WINDOW, :] = jnp.concatenate(finished[b], axis=1)
    ways = len(outs) // 2
    own = rows // ways
    blocks = [out_ref[pl.ds(pl.multiple_of((tp_ref[0] ^ m) * own, 16), own), :] for m in range(ways)]
    for m in range(ways):
        outs[m][...] = blocks[m]
        for n in range(1, ways):
            outs[ways + m][(n - 1) * own : n * own] = blocks[m ^ n]


def mixed_and_normed(residual, parts, weight, gain):
    mixed = (residual.astype(F32) + dot32(parts, weight)).astype(BF)
    wide = mixed.astype(F32)
    scale = lax.rsqrt(jnp.mean(wide * wide, axis=1, keepdims=True) + NORM_EPSILON)
    return mixed, (wide * scale * gain).astype(BF)


def block_ids(ids_ref, block, own):
    rows = ids_ref.shape[1]
    return pltpu.roll(ids_ref[...], lax.rem(rows - block * own, rows), 1)[:, :own]


def ranks_of(ids, experts):
    own = ids.shape[1]
    expert_index = lax.broadcasted_iota(jnp.int32, (experts, own), 0)
    named = expert_index == ids[0:1, :]
    for k in range(1, ids.shape[0]):
        named = named | (expert_index == ids[k : k + 1, :])
    ones = jnp.where(named, 1.0, 0.0).astype(BF)
    earlier = jnp.where(
        lax.broadcasted_iota(jnp.int32, (own, own), 0)
        < lax.broadcasted_iota(jnp.int32, (own, own), 1),
        1.0,
        0.0,
    ).astype(BF)
    return jnp.where(named, dot32(ones, earlier), -1.0).astype(BF)


def slot_choice(ranks, place, rank, turn, experts_here, c):
    experts = ranks.shape[0]
    wanted = (place ^ turn) * experts_here + c
    shape = (place.shape[0], experts)
    pick = jnp.where(lax.broadcasted_iota(jnp.int32, shape, 1) == wanted, 1.0, 0.0).astype(BF)
    return jnp.where(dot32(pick, ranks) == rank, 1.0, 0.0).astype(BF)


def dispatch_body(ways, tp_ref, turn_ref, *refs, experts):
    parts, (residual_ref, weight_ref, gain_ref, ids_ref, place_ref, rank_ref) = (
        refs[:ways],
        refs[ways : ways + 6],
    )
    mixed_ref, slot_refs = refs[ways + 6], refs[ways + 7 :]
    own = mixed_ref.shape[0]
    parts = jnp.concatenate([part[...] for part in parts], axis=1)
    mixed, normed = mixed_and_normed(
        residual_ref[:own], parts, weight_ref[...], gain_ref[...]
    )
    mixed_ref[...] = mixed
    ranks = ranks_of(block_ids(ids_ref, tp_ref[0], own), experts[0])
    chosen = slot_choice(ranks, place_ref[...], rank_ref[...], turn_ref[0], experts[1], 0)
    result = dot32(chosen, normed)
    for p, slot_ref in enumerate(slot_refs):
        count = slot_ref.shape[0]
        slot_ref[...] = result[p * count : (p + 1) * count].astype(BF)


def gated(x, gate, up):
    gate_values = dot32(x, gate)
    up_values = dot32(x, up)
    return (gate_values / (1.0 + jnp.exp(-gate_values)) * up_values).astype(BF)


def second_body(ways, tp_ref, turn_ref, *refs, experts):
    parts, rests = refs[:ways], refs[ways : 2 * ways]
    residual_ref, weight_ref, gain_ref, ids_ref, place_ref, rank_ref = refs[
        2 * ways : 2 * ways + 6
    ]
    slot_refs = refs[2 * ways + 6 :]
    own = residual_ref.shape[0] // ways
    blocks, residual = [], []
    for m in range(0, ways, 2):
        rows = [rest[(m - 1) * own : m * own] for rest in rests] if m else [
            part[...] for part in parts
        ]
        blocks.append(jnp.concatenate(rows, axis=1))
        residual.append(residual_ref[m * own : (m + 1) * own])
    blocks, residual = jnp.concatenate(blocks, axis=0), jnp.concatenate(residual, axis=0)
    _, normed = mixed_and_normed(residual, blocks, weight_ref[...], gain_ref[...])
    pieces = len(slot_refs) // (experts[1] - 1)
    for m in range(0, ways, 2):
        ranks = ranks_of(block_ids(ids_ref, tp_ref[0] ^ m, own), experts[0])
        rows = normed[(m // 2) * own : (m // 2 + 1) * own]
        for c in range(1, experts[1]):
            chosen = slot_choice(
                ranks, place_ref[...], rank_ref[...], turn_ref[0], experts[1], c
            )
            result = dot32(chosen, rows)
            for p in range(pieces):
                slots_ref = slot_refs[(c - 1) * pieces + p]
                count = slots_ref.shape[0] // (ways // 2)
                slots_ref[(m // 2) * count : (m // 2 + 1) * count] = result[
                    p * count : (p + 1) * count
                ].astype(BF)


def shared_body(ways, *refs):
    parts, rests = refs[:ways], refs[ways : 2 * ways]
    residual_ref, weight_ref, gain_ref, gate_ref, up_ref, down_ref = refs[
        2 * ways : 2 * ways + 6
    ]
    keep_ref, send_ref = refs[2 * ways + 6 :]
    own = keep_ref.shape[1]
    rows = [
        jnp.concatenate([part[...], rest[...]], axis=0) for part, rest in zip(parts, rests)
    ]
    _, normed = mixed_and_normed(
        residual_ref[...], jnp.concatenate(rows, axis=1), weight_ref[...], gain_ref[...]
    )
    hidden = gated(normed, gate_ref[...], up_ref[...])
    result = dot32(hidden, down_ref[...]).astype(BF)
    for m in range(ways):
        target = keep_ref if m % 2 == 0 else send_ref
        target[m // 2] = result[m * own : (m + 1) * own]


def expert_body(c, count, *refs):
    gate_ref, up_ref, down_ref = refs[count : count + 3]
    for x_ref, out_ref in zip(refs[:count], refs[count + 3 :]):
        hidden = gated(x_ref[...], gate_ref[c], up_ref[c])
        out_ref[...] = dot32(hidden, down_ref[c]).astype(BF)


def expert_rows(c, xs, gates, ups, downs):
    rows, width = xs[0].shape
    hid = gates.shape[2]
    count = len(xs)
    return call(
        functools.partial(expert_body, c, count),
        [((rows, width), BF)] * count,
        (*xs, gates, ups, downs),
        flops=6 * rows * width * hid * count,
        moved=4 * rows * width * count + 6 * width * hid,
    )


def marker_body(x_ref, out_ref):
    out_ref[...] = x_ref[...]


def marker(x):
    return call(marker_body, [(x.shape, x.dtype)], (x,), flops=1000, moved=1000)[0]


def joined_body(count, *refs):
    pieces, outs = refs[:count], refs[count:]
    rows = outs[0].shape[0] // count
    for p, piece in enumerate(pieces):
        for h, out in enumerate(outs):
            out[p * rows : (p + 1) * rows] = piece[h * rows : (h + 1) * rows]


def joined(pieces, halves=1):
    rows, width = pieces[0].shape
    count = len(pieces)
    return call(
        functools.partial(joined_body, count),
        [((count * rows // halves, width), BF)] * halves,
        pieces,
        flops=rows * width * count,
        moved=4 * rows * width * count,
    )


def prepare_body(
    tp_ref, turn_ref, ids_ref, route_ref, place_ref, rank_ref, *out_refs, experts,
):
    own = route_ref.shape[1]
    ids = block_ids(ids_ref, tp_ref[0], own)
    ranks = ranks_of(ids, experts[0])
    expert_index = lax.broadcasted_iota(jnp.int32, (experts[0], own), 0)
    weight = jnp.zeros((experts[0], own), F32)
    for k in range(ids.shape[0]):
        weight = weight + jnp.where(
            expert_index == ids[k : k + 1, :], route_ref[k : k + 1, :], 0.0
        )
    upper = weight.astype(BF)
    lower = (weight - upper.astype(F32)).astype(BF)
    row_index = lax.broadcasted_iota(jnp.int32, (experts[0], place_ref.shape[1]), 0)

    def spread(x, pick):
        return lax.dot_general(x, pick, (((0,), (0,)), ((), ())), preferred_element_type=F32)

    for c, out_ref in enumerate(out_refs):
        wanted = (place_ref[...] ^ turn_ref[0]) * experts[1] + c
        pick = jnp.where(row_index == wanted, 1.0, 0.0).astype(BF)
        chosen = spread(ranks, pick) == rank_ref[...]
        out_ref[0] = jnp.where(chosen, spread(upper, pick), 0.0).astype(BF)
        out_ref[1] = jnp.where(chosen, spread(lower, pick), 0.0).astype(BF)


def load_body(count, ways, tp_ref, *refs):
    sources, outs, sems = refs[:count], refs[-1 - count : -1], refs[-1]
    copies = []
    for source, out in zip(sources, outs):
        rows = source.shape[0] // ways
        for m in range(ways):
            cut = (
                pl.ds(pl.multiple_of((tp_ref[0] ^ m) * rows, 16), rows) if ways > 1 else pl.ds(0, rows)
            )
            copies.append(
                pltpu.make_async_copy(
                    source.at[cut], out.at[pl.ds(m * rows, rows)], sems.at[len(copies)]
                )
            )
    for copy in copies:
        copy.start()
    for copy in copies:
        copy.wait()


def load(arrays, after, tp, ways):
    hbm = pl.BlockSpec(memory_space=pltpu.HBM)
    return pl.pallas_call(
        functools.partial(load_body, len(arrays), ways),
        out_shape=[pltpu.VMEM(x.shape, x.dtype) for x in arrays],
        grid_spec=pltpu.PrefetchScalarGridSpec(
            num_scalar_prefetch=1,
            grid=(),
            in_specs=[hbm] * (len(arrays) + len(after)),
            out_specs=[pl.BlockSpec(memory_space=pltpu.VMEM)] * len(arrays),
            scratch_shapes=[pltpu.SemaphoreType.DMA((len(arrays) * ways,))],
        ),
        compiler_params=pltpu.CompilerParams(vmem_limit_bytes=1024 * 1024),
        cost_estimate=pl.CostEstimate(
            flops=1000, bytes_accessed=sum(2 * x.size for x in arrays), transcendentals=0
        ),
    )(tp, *(pltpu.with_memory_space_constraint(x, pltpu.HBM) for x in (*arrays, *after)))


def combine_body(count, weights_ref, *refs):
    back_ref = refs[-1]
    rows = back_ref.shape[0] // count
    for p in range(count):
        back_ref[p * rows : (p + 1) * rows] = refs[p][...]
    back = back_ref[...]
    total = dot32(weights_ref[0], back) + dot32(weights_ref[1], back)
    for ref in refs[count:-2]:
        total = total + ref[...].astype(F32)
    refs[-2][...] = total.astype(refs[-2].dtype)


def layer(
    queries,
    keys,
    values,
    sinks,
    residual,
    out_weight,
    norm_gain,
    shared_gate,
    shared_up,
    shared_down,
    expert_ids,
    route_weights,
    expert_gate,
    expert_up,
    expert_down,
):
    block_rows, query_width = queries.shape
    ways = lax.axis_size("tp")
    splits = lax.axis_size("sp")
    width_index = lax.axis_index("tp")
    sp_index = lax.axis_index("sp")
    model_width = out_weight.shape[1]
    own = block_rows // ways
    halves = ways // 2
    experts_here = expert_gate.shape[0]
    experts_all = experts_here * splits
    capacity = max(2, 2 * own * TOPK // experts_all)
    slots = splits * capacity
    turning = splits <= 8
    half = splits // 2

    def over(x, mask):
        return lax.ppermute(x, "tp", [(i, i ^ mask) for i in range(ways)])

    def exchange(x):
        return lax.all_to_all(x, "sp", 0, 0, tiled=True)

    def turned(pieces, masks):
        done = []
        for piece, m in zip(pieces, masks):
            pairs = [(i, i ^ m) for i in range(splits)]
            done.append(lax.ppermute(piece, "sp", pairs) if m else piece)
        return done

    def plus(a, b):
        return (a.astype(F32) + b.astype(F32)).astype(BF)

    def returned(keep, send):
        if not turning:
            keep, send = jnp.concatenate(keep, axis=0), jnp.concatenate(send, axis=0)
            return [exchange(plus(keep, over(send, 2)))]
        pieces = []
        for part in (1, 0):
            other = over(send[part], 2)
            if part == 0:
                other, summed = lax.optimization_barrier((other, summed))
            summed = plus(keep[part], other)
            masks = range(part * half, (part + 1) * half)
            sent = [summed[k * capacity : (k + 1) * capacity] for k in range(half)]
            pieces = turned(sent, masks) + pieces
        return pieces

    up = [(i, i + 1) for i in range(splits - 1)]
    down = [(i + 1, i) for i in range(splits - 1)]
    keys_t, values_t = keys.T, values.T
    tail = jnp.concatenate([keys_t[:, -WINDOW:], values_t[:, -WINDOW:]], axis=0)
    head = jnp.concatenate([keys_t[:, :WINDOW], values_t[:, :WINDOW]], axis=0)
    tp = width_index.reshape(1)
    gain = norm_gain.reshape(1, model_width)
    ids_t = expert_ids.T
    experts = (experts_all, experts_here)
    place = np.arange(slots, dtype=np.int32) // capacity
    rank = (np.arange(slots) % capacity).astype(np.float32)
    turn = (sp_index if turning else sp_index * 0).reshape(1)
    before = lax.ppermute(tail, "sp", up)
    after = lax.ppermute(head, "sp", down)
    quarter = HEAD_DIM // 4
    spectrum = ROPE_BASE ** (-np.arange(quarter, dtype=np.float64) / quarter)
    spectrum = np.concatenate([spectrum, spectrum])[:, None].astype(np.float32)
    attended = call(
        functools.partial(attention_body, total_rows=splits * block_rows),
        [((own, query_width), BF)] * ways + [((block_rows - own, query_width), BF)] * ways,
        (queries.T, keys_t, values_t, before, after, jnp.asarray(spectrum)),
        scalars=(tp, sp_index.reshape(1), sinks),
        scratch=[
            pltpu.VMEM((block_rows, query_width), BF),
            pltpu.VMEM((block_rows + 2 * WINDOW, HEAD_DIM), BF),
            pltpu.VMEM((HEAD_DIM, block_rows + 2 * WINDOW), BF),
        ],
        flops=12 * block_rows * WINDOW * query_width,
        moved=4 * block_rows * query_width,
    )

    combine_weights = call(
        functools.partial(prepare_body, experts=experts),
        [((2, own, slots), BF)] * experts_here,
        (
            ids_t,
            route_weights.T,
            jnp.asarray(place[None, :]),
            jnp.asarray(rank[None, :]),
        ),
        scalars=(tp, turn),
        flops=8 * own * experts_all * slots,
        moved=8 * own * slots,
    )
    out_weight, residual = load((out_weight, residual), (turn,), tp, ways)
    parts = [over(attended[m], m) if m else attended[m] for m in range(ways)]
    rests = [over(attended[ways + m], m) if m else attended[ways + m] for m in range(ways)]
    mixed, *outgoing = call(
        functools.partial(dispatch_body, ways, experts=experts),
        [((own, model_width), BF)] + [((capacity, model_width), BF)] * splits,
        (
            *parts,
            residual,
            out_weight,
            gain,
            ids_t,
            jnp.asarray(place[:, None]),
            jnp.asarray(rank[:, None]),
        ),
        scalars=(tp, turn),
        flops=2 * own * model_width * (out_weight.shape[0] + slots),
        moved=2 * out_weight.size,
    )
    if turning:
        arrived = turned(outgoing, range(splits))
        near = []
        for part in range(2):
            near += joined(arrived[part * half : (part + 1) * half])
    else:
        near = exchange(jnp.concatenate(outgoing, axis=0))
        near = [near[: half * capacity], near[half * capacity :]]
    gain_late = marker(gain)
    combine_weights = [marker(x) for x in combine_weights]

    outgoing = call(
        functools.partial(second_body, ways, experts=experts),
        [((halves * capacity, model_width), BF)] * (splits * (experts_here - 1)),
        (
            *parts,
            *rests,
            residual,
            out_weight,
            gain,
            ids_t,
            jnp.asarray(place[:, None]),
            jnp.asarray(rank[:, None]),
        ),
        scalars=(tp, turn),
        flops=2 * halves * own * model_width * (out_weight.shape[0] + slots),
        moved=2 * out_weight.size,
    )
    sources = (shared_gate, shared_up, shared_down, expert_gate, expert_up, expert_down)
    shared_gate, shared_up, shared_down, *weights = load(sources, (gain_late,), tp, 1)
    keep, send = call(
        functools.partial(shared_body, ways),
        [((halves, own, model_width), BF)] * 2,
        (
            *parts,
            *rests,
            residual,
            out_weight,
            gain_late,
            shared_gate,
            shared_up,
            shared_down,
        ),
        flops=2 * block_rows * model_width * (out_weight.shape[0] + 3 * shared_gate.shape[1]),
        moved=2 * out_weight.size,
    )
    got = over(send, 1)
    shared_own = plus(keep[0], got[0])
    shared_far = over(plus(keep[1], got[1]), 2)

    far_sums, pairs = [None] * 2, [None] * 2
    for part in (1, 0):
        far = over(near[part], 2)
        pairs[part] = over(near[part], 1)
        far_pair = over(far, 1)
        out_pair, out_far = expert_rows(0, [far_pair, far], *weights)
        out_pair = over(out_pair, 1)
        far_sums[part] = plus(out_far, out_pair)
    outs = expert_rows(0, [*pairs, *near], *weights)
    near_sums = [plus(outs[2 + p], over(outs[p], 1)) for p in range(2)]
    back = [returned(near_sums, far_sums)]

    for c in range(1, experts_here):
        pieces = outgoing[splits * (c - 1) : splits * c]
        if turning:
            arrived = turned(pieces, range(splits))
            mine, far = joined(arrived, halves)
        else:
            arrived = exchange(jnp.concatenate(pieces, axis=0))
            arrived = arrived.reshape(splits, halves, capacity, model_width)
            mine, far = (arrived[:, h].reshape(slots, model_width) for h in range(halves))
        far_pair = over(far, 1)
        out_pair, out_far = expert_rows(c, [far_pair, far], *weights)
        far_sum = plus(out_far, over(out_pair, 1))
        pair = over(mine, 1)
        out_pair, out_mine = expert_rows(c, [pair, mine], *weights)
        summed = plus(out_mine, over(out_pair, 1))
        cut = half * capacity
        summed, far_sum = ([x[:cut], x[cut:]] for x in (summed, far_sum))
        back.append(returned(summed, far_sum))

    total = None
    for c in range(experts_here):
        last = c == experts_here - 1
        added = (mixed, shared_own, shared_far) if total is None else (total,)
        total = call(
            functools.partial(combine_body, len(back[c])),
            [((own, model_width), BF if last else F32)],
            (combine_weights[c], *back[c], *added),
            scratch=[pltpu.VMEM((slots, model_width), BF)],
            final=last,
            flops=4 * own * slots * model_width,
            moved=2 * slots * model_width,
        )[0]
    return total


def solution(mesh):
    placed = (
        P("sp", "tp"),
        P("sp", "tp"),
        P("sp", "tp"),
        P("tp"),
        P("sp", None),
        P(),
        P(),
        P(None, "tp"),
        P(None, "tp"),
        P("tp", None),
        P("sp", None),
        P(("sp", "tp"), None),
        P("sp", None, "tp"),
        P("sp", None, "tp"),
        P("sp", "tp", None),
    )
    return jax.shard_map(
        layer, mesh=mesh, in_specs=placed, out_specs=P(("sp", "tp"), None), check_vma=False
    )
```

time: 215 us -> 192 us (0.89)
  Pallas kernels: 55.6 us -> 24.9 us
  starting transfers between devices: 57.7 us -> 79.1 us
  blocking collectives: 9.27 us -> 0 us
  local copies, waits for them, and re-layouts: 10.3 us -> 6.16 us
    pallas_call x13 -> x20, Pallas kernels: 55.6 us -> 24.9 us  [the longest x18 19.2 us: call(): pl.pallas_call(body, out_shape=[shape_of(shape, kind) for shape, kind in...]
    ppermute x21 -> x28, starting transfers between devices: 34.8 us -> 55.9 us  [turned(): done.append(lax.ppermute(piece, 'sp', pairs) if m else piece)]
    ppermute x15 -> x26, starting transfers between devices: 6.93 us -> 17 us  [over(): return lax.ppermute(x, 'tp', [(i, i ^ mask) for i in range(ways)])]
    all_to_all x1 -> x0, starting transfers between devices: 9.85 us -> none  [exchange(): return lax.all_to_all(x, 'sp', 0, 0, tiled=True)]
    all_gather x1 -> x0, blocking collectives: 9.27 us -> none  [layer(): parts = lax.all_gather(attended, 'tp', axis=0, tiled=False)]
    all_to_all x1 -> x0, waiting for transfers between devices: 7.52 us -> none  [exchange(): return lax.all_to_all(x, 'sp', 0, 0, tiled=True)]
    ppermute x15 -> x26, waiting for transfers between devices: 39.5 us -> 44.3 us  [over(): return lax.ppermute(x, 'tp', [(i, i ^ mask) for i in range(ways)])]
    ppermute x21 -> x28, waiting for transfers between devices: 28.4 us -> 30 us  [turned(): done.append(lax.ppermute(piece, 'sp', pairs) if m else piece)]
  transfers between devices with their start and end apart: 39 -> 56, of which waited for: 11 -> 18; matrix products, arithmetic and copies ran while one was open for 3% -> 1% of each run, Pallas kernels for 19% -> 11%
where the time goes in v1:
time: 192 us; the launch traced here: 191 us
  starting transfers between devices  79.1 us (41%)
  waiting for transfers between devices  78.8 us (41%)
  Pallas kernels  24.9 us (13%)
  local copies, waits for them, and re-layouts  6.16 us (3%)
    ppermute x28, starting transfers between devices, turned(): done.append(lax.ppermute(piece, 'sp', pairs) if m else piece)  55.9 us
    ppermute x26, waiting for transfers between devices, over(): return lax.ppermute(x, 'tp', [(i, i ^ mask) for i in range(ways)])  44.3 us
    ppermute x28, waiting for transfers between devices, turned(): done.append(lax.ppermute(piece, 'sp', pairs) if m else piece)  30 us
    pallas_call x18, Pallas kernels, call(): pl.pallas_call(body, out_shape=[shape_of(shape, kind) for shape, kind in...  19.2 us
    ppermute x26, starting transfers between devices, over(): return lax.ppermute(x, 'tp', [(i, i ^ mask) for i in range(ways)])  17 us
    pallas_call x2, Pallas kernels, load(): pl.pallas_call(functools.partial(load_body, len(arrays), ways), out_shape...  5.75 us
    unnamed x28, local copies, waits for them, and re-layouts  5.21 us
    ppermute x1, starting transfers between devices, layer(): before = lax.ppermute(tail, 'sp', up)  4.87 us
  transfers between devices with their start and end apart: 56, of which 18 were waited for; matrix products, arithmetic and copies ran while one was open for 1% of the time, Pallas kernels for 11%

profile of v1, /device:TPU:0, one launch (start us, length us, event | category | flops | bytes accessed | tf_op | source)
XLA Modules:
  0.0 191.2 jit_solution(5892872391636928940)
XLA Ops:
  0.8 4.9 %collective-permute-start = (bf16[128,128]{1,0:T(8,128)(2,1)S(1)}, bf16[128,128]{1,0:T(8,128)(2,1)S(1)}, u32[]{:S(2)}, u32[]{:S(2)}) collective-permute-start(bf16[128,128]{1,0:T(8,128)(2,1)S(1)} %pad_maximum_fusion), channel_id=1, source_target_pairs={{0,4},{4,8},{8,12},{12,16},{16,20},{20,24},{24,28},{1,5},{5,9},{9,... | collective-permute-start | bytes 98312 | tf_op jit(solution)/shard_map/ppermute | solution.py:444
  7.2 4.2 %collective-permute-done.1.after_ref = bf16[128,128]{1,0:T(8,128)(2,1)S(1)} collective-permute-done((bf16[128,128]{1,0:T(8,128)(2,1)S(1)}, bf16[128,128]{1,0:T(8,128)(2,1)S(1)}, u32[]{:S(2)}, u32[]{:S(2)}) %collective-permute-start.1) | collective-permute-done | bytes 32800 | tf_op jit(solution)/shard_map/ppermute | solution.py:445
  15.4 2.6 %shard_map.210 = (bf16[96,192]{1,0:T(8,128)(2,1)S(1)}, bf16[96,192]{1,0:T(8,128)(2,1)S(1)}, bf16[96,192]{1,0:T(8,128)(2,1)S(1)}, bf16[96,192]{1,0:T(8,128)(2,1)S...) custom-call(s32[1]{0:T(128)} %bitcast.tp_ref, ...), custom_call_target="tpu_custom_call" | custom-call | flops 113246208 | bytes 294912 | tf_op jit(solution)/shard_map/pallas_call | solution.py:38
  22.7 2.4 %shard_map.211 = (bf16[768,2048]{1,0:T(8,128)(2,1)S(1)}, bf16[384,2048]{1,0:T(8,128)(2,1)S(1)}) custom-call(s32[1]{0:T(128)} %bitcast.tp_ref, bf16[768,2048]{1,0:T(8,128)(2,1)} %refs_0_.2, bf16[384,2048]{1,0:T(8,128)(2,1)} %refs_1_.2, s32[1]{0:T(128)} %bitcast.1.turn_ref.first_ref.refs_2_), custom_call_target="tpu_custom_call" | custom-call | flops 1000 | bytes 4718592 | tf_op jit(solution)/shard_map/pallas_call | solution.py:340
  25.0 4.0 %collective-permute-done.3.refs_2_ = bf16[96,192]{1,0:T(8,128)(2,1)S(1)} collective-permute-done((bf16[96,192]{1,0:T(8,128)(2,1)S(1)}, bf16[96,192]{1,0:T(8,128)(2,1)S(1)}, u32[]{:S(2)}, u32[]{:S(2)}) %collective-permute-start.3) | collective-permute-done | bytes 36896 | tf_op jit(solution)/shard_map/ppermute | solution.py:402
  30.2 2.7 %collective-permute-start.32 = (bf16[24,2048]{1,0:T(8,128)(2,1)S(1)}, bf16[24,2048]{1,0:T(8,128)(2,1)S(1)}, u32[]{:S(2)}, u32[]{:S(2)}) collective-permute-start(bf16[24,2048]{1,0:T(8,128)(2,1)S(1)} %get-tuple-element.92), channel_id=1, source_target_pairs={{0,16},{4,20},{8,24},{12,28},{16,0},{20,4},{24,8},{28,12},{1,17},{... | collective-permute-start | bytes 294920 | tf_op jit(solution)/shard_map/ppermute | solution.py:411
  32.9 2.2 %collective-permute-start.33 = (bf16[24,2048]{1,0:T(8,128)(2,1)S(1)}, bf16[24,2048]{1,0:T(8,128)(2,1)S(1)}, u32[]{:S(2)}, u32[]{:S(2)}) collective-permute-start(bf16[24,2048]{1,0:T(8,128)(2,1)S(1)} %get-tuple-element.93), channel_id=1, source_target_pairs={{0,20},{4,16},{8,28},{12,24},{16,4},{20,0},{24,12},{28,8},{1,21},{... | collective-permute-start | bytes 294920 | tf_op jit(solution)/shard_map/ppermute | solution.py:411
  39.1 3.2 %collective-permute-start.35 = (bf16[24,2048]{1,0:T(8,128)(2,1)S(1)}, bf16[24,2048]{1,0:T(8,128)(2,1)S(1)}, u32[]{:S(2)}, u32[]{:S(2)}) collective-permute-start(bf16[24,2048]{1,0:T(8,128)(2,1)S(1)} %get-tuple-element.95), channel_id=1, source_target_pairs={{0,28},{4,24},{8,20},{12,16},{16,12},{20,8},{24,4},{28,0},{1,29},{... | collective-permute-start | bytes 294920 | tf_op jit(solution)/shard_map/ppermute | solution.py:411
  43.3 2.5 %collective-permute-start.28 = (bf16[24,2048]{1,0:T(8,128)(2,1)S(1)}, bf16[24,2048]{1,0:T(8,128)(2,1)S(1)}, u32[]{:S(2)}, u32[]{:S(2)}) collective-permute-start(bf16[24,2048]{1,0:T(8,128)(2,1)S(1)} %get-tuple-element.89), channel_id=1, source_target_pairs={{0,4},{4,0},{8,12},{12,8},{16,20},{20,16},{24,28},{28,24},{1,5},{5... | collective-permute-start | bytes 294920 | tf_op jit(solution)/shard_map/ppermute | solution.py:411
  47.5 4.5 %collective-permute-start.30 = (bf16[24,2048]{1,0:T(8,128)(2,1)S(1)}, bf16[24,2048]{1,0:T(8,128)(2,1)S(1)}, u32[]{:S(2)}, u32[]{:S(2)}) collective-permute-start(bf16[24,2048]{1,0:T(8,128)(2,1)S(1)} %get-tuple-element.91), channel_id=1, source_target_pairs={{0,12},{4,8},{8,4},{12,0},{16,28},{20,24},{24,20},{28,16},{1,13},{... | collective-permute-start | bytes 294920 | tf_op jit(solution)/shard_map/ppermute | solution.py:411
  53.9 3.4 %shard_map.215 = (bf16[2048,128]{1,0:T(8,128)(2,1)S(1)}, bf16[2048,128]{1,0:T(8,128)(2,1)S(1)}, bf16[128,2048]{1,0:T(8,128)(2,1)S(1)}, bf16[2,2048,256]{2,1,0:T(...) custom-call(s32[1]{0:T(128)} %bitcast.tp_ref, bf16[2048,128]{1,0:T(8,128)(2,1)} %refs_0_.3, ...), custom_call_target="tpu_custom_call" | custom-call | flops 1000 | bytes 7864320 | tf_op jit(solution)/shard_map/pallas_call | solution.py:340
  57.4 2.2 %collective-permute-start.12 = (bf16[48,2048]{1,0:T(8,128)(2,1)S(1)}, bf16[48,2048]{1,0:T(8,128)(2,1)S(1)}, u32[]{:S(2)}, u32[]{:S(2)}) collective-permute-start(bf16[48,2048]{1,0:T(8,128)(2,1)S(1)} %get-tuple-element.74), channel_id=1, source_target_pairs={{0,20},{4,16},{8,28},{12,24},{16,4},{20,0},{24,12},{28,8},{1,21},{... | collective-permute-start | bytes 589832 | tf_op jit(solution)/shard_map/ppermute | solution.py:411
  61.0 2.8 %collective-permute-start.14 = (bf16[48,2048]{1,0:T(8,128)(2,1)S(1)}, bf16[48,2048]{1,0:T(8,128)(2,1)S(1)}, u32[]{:S(2)}, u32[]{:S(2)}) collective-permute-start(bf16[48,2048]{1,0:T(8,128)(2,1)S(1)} %get-tuple-element.76), channel_id=1, source_target_pairs={{0,28},{4,24},{8,20},{12,16},{16,12},{20,8},{24,4},{28,0},{1,29},{... | collective-permute-start | bytes 589832 | tf_op jit(solution)/shard_map/ppermute | solution.py:411
  66.0 3.0 %shard_map.225 = (bf16[2,96,2048]{2,1,0:T(8,128)(2,1)S(1)}, bf16[2,96,2048]{2,1,0:T(8,128)(2,1)S(1)}) custom-call(bf16[96,192]{1,0:T(8,128)(2,1)S(1)} %get-tuple-element.59.refs_0_, bf16[96,192]{1,0:T(8,128)(2,1)S(1)} %collective-permute-done.2.refs_1_, bf16[96,192]{1,0:T(8,128)(2,1)S(1)} %collective-permute-done.3.refs_2_, ...), custom_call_target="tpu_custom_call" | custom-call | flops 1811939328 | bytes 3145728 | tf_op jit(solution)/shard_map/pallas_call | solution.py:38
  69.0 7.6 %collective-permute-done.11.refs_4_ = bf16[48,2048]{1,0:T(8,128)(2,1)S(1)} collective-permute-done((bf16[48,2048]{1,0:T(8,128)(2,1)S(1)}, bf16[48,2048]{1,0:T(8,128)(2,1)S(1)}, u32[]{:S(2)}, u32[]{:S(2)}) %collective-permute-start.11) | collective-permute-done | bytes 196640 | tf_op jit(solution)/shard_map/ppermute | solution.py:411
  76.6 5.0 %collective-permute-done.12.refs_5_ = bf16[48,2048]{1,0:T(8,128)(2,1)S(1)} collective-permute-done((bf16[48,2048]{1,0:T(8,128)(2,1)S(1)}, bf16[48,2048]{1,0:T(8,128)(2,1)S(1)}, u32[]{:S(2)}, u32[]{:S(2)}) %collective-permute-start.12) | collective-permute-done | bytes 196640 | tf_op jit(solution)/shard_map/ppermute | solution.py:411
  82.3 3.3 %collective-permute-start.9 = (bf16[48,2048]{1,0:T(8,128)(2,1)S(1)}, bf16[48,2048]{1,0:T(8,128)(2,1)S(1)}, u32[]{:S(2)}, u32[]{:S(2)}) collective-permute-start(bf16[48,2048]{1,0:T(8,128)(2,1)S(1)} %get-tuple-element.71), channel_id=1, source_target_pairs={{0,8},{4,12},{8,0},{12,4},{16,24},{20,28},{24,16},{28,20},{1,9},{5... | collective-permute-start | bytes 589832 | tf_op jit(solution)/shard_map/ppermute | solution.py:411
  91.6 2.5 %shard_map.222 = (bf16[96,2048]{1,0:T(8,128)(2,1)S(1)}, bf16[96,2048]{1,0:T(8,128)(2,1)S(1)}, bf16[96,2048]{1,0:T(8,128)(2,1)S(1)}, bf16[96,2048]{1,0:T(8,128)(2,1)S(1)}) custom-call(bf16[96,2048]{1,0:T(8,128)(2,1)S(1)} %collective-permute-done.31.refs_0_, bf16[96,2048]{1,0:T(8,128)(2,1)S(1)} %collective-permute-done.36.refs_1_, ...), custom_call_target="tpu_custom_call" | custom-call | flops 1207959552 | bytes 6291456 | tf_op jit(solution)/shard_map/pallas_call | solution.py:38
  94.1 4.9 %collective-permute-done.38.refs_1_ = bf16[96,2048]{1,0:T(8,128)(2,1)S(1)} collective-permute-done((bf16[96,2048]{1,0:T(8,128)(2,1)S(1)}, bf16[96,2048]{1,0:T(8,128)(2,1)S(1)}, u32[]{:S(2)}, u32[]{:S(2)}) %collective-permute-start.38) | collective-permute-done | bytes 393248 | tf_op jit(solution)/shard_map/ppermute | solution.py:402
  109.7 13.1 %collective-permute-done.46 = bf16[96,2048]{1,0:T(8,128)(2,1)S(1)} collective-permute-done((bf16[96,2048]{1,0:T(8,128)(2,1)S(1)}, bf16[96,2048]{1,0:T(8,128)(2,1)S(1)}, u32[]{:S(2)}, u32[]{:S(2)}) %collective-permute-start.46) | collective-permute-done | bytes 393248 | tf_op jit(solution)/shard_map/ppermute | solution.py:402
  124.6 8.5 %collective-permute-done.41 = bf16[96,2048]{1,0:T(8,128)(2,1)S(1)} collective-permute-done((bf16[96,2048]{1,0:T(8,128)(2,1)S(1)}, bf16[96,2048]{1,0:T(8,128)(2,1)S(1)}, u32[]{:S(2)}, u32[]{:S(2)}) %collective-permute-start.41) | collective-permute-done | bytes 393248 | tf_op jit(solution)/shard_map/ppermute | solution.py:402
  139.9 7.4 %collective-permute-done.20 = bf16[96,2048]{1,0:T(8,128)(2,1)S(1)} collective-permute-done((bf16[96,2048]{1,0:T(8,128)(2,1)S(1)}, bf16[96,2048]{1,0:T(8,128)(2,1)S(1)}, u32[]{:S(2)}, u32[]{:S(2)}) %collective-permute-start.20) | collective-permute-done | bytes 393248 | tf_op jit(solution)/shard_map/ppermute | solution.py:402
  149.0 6.3 %collective-permute-done.19 = bf16[96,2048]{1,0:T(8,128)(2,1)S(1)} collective-permute-done((bf16[96,2048]{1,0:T(8,128)(2,1)S(1)}, bf16[96,2048]{1,0:T(8,128)(2,1)S(1)}, u32[]{:S(2)}, u32[]{:S(2)}) %collective-permute-start.19) | collective-permute-done | bytes 393248 | tf_op jit(solution)/shard_map/ppermute | solution.py:402
  158.6 2.3 %collective-permute-start.52 = (bf16[24,2048]{1,0:T(8,128)(2,1)S(1)}, bf16[24,2048]{1,0:T(8,128)(2,1)S(1)}, u32[]{:S(2)}, u32[]{:S(2)}) collective-permute-start(bf16[24,2048]{1,0:T(8,128)(2,1)S(1)} %get-tuple-element.116), channel_id=1, source_target_pairs={{0,24},{4,28},{8,16},{12,20},{16,8},{20,12},{24,0},{28,4},{1,25},{... | collective-permute-start | bytes 294920 | tf_op jit(solution)/shard_map/ppermute | solution.py:411
  160.9 2.3 %collective-permute-start.53 = (bf16[24,2048]{1,0:T(8,128)(2,1)S(1)}, bf16[24,2048]{1,0:T(8,128)(2,1)S(1)}, u32[]{:S(2)}, u32[]{:S(2)}) collective-permute-start(bf16[24,2048]{1,0:T(8,128)(2,1)S(1)} %get-tuple-element.115), channel_id=1, source_target_pairs={{0,28},{4,24},{8,20},{12,16},{16,12},{20,8},{24,4},{28,0},{1,29},{... | collective-permute-start | bytes 294920 | tf_op jit(solution)/shard_map/ppermute | solution.py:411
  163.9 2.0 %collective-permute-done.50.refs_4_ = bf16[24,2048]{1,0:T(8,128)(2,1)S(1)} collective-permute-done((bf16[24,2048]{1,0:T(8,128)(2,1)S(1)}, bf16[24,2048]{1,0:T(8,128)(2,1)S(1)}, u32[]{:S(2)}, u32[]{:S(2)}) %collective-permute-start.50) | collective-permute-done | bytes 98336 | tf_op jit(solution)/shard_map/ppermute | solution.py:411
  165.9 5.0 %collective-permute-done.51.refs_5_ = bf16[24,2048]{1,0:T(8,128)(2,1)S(1)} collective-permute-done((bf16[24,2048]{1,0:T(8,128)(2,1)S(1)}, bf16[24,2048]{1,0:T(8,128)(2,1)S(1)}, u32[]{:S(2)}, u32[]{:S(2)}) %collective-permute-start.51) | collective-permute-done | bytes 98336 | tf_op jit(solution)/shard_map/ppermute | solution.py:411
  170.9 2.0 %collective-permute-start.24 = (bf16[24,2048]{1,0:T(8,128)(2,1)S(1)}, bf16[24,2048]{1,0:T(8,128)(2,1)S(1)}, u32[]{:S(2)}, u32[]{:S(2)}) collective-permute-start(bf16[24,2048]{1,0:T(8,128)(2,1)S(1)} %get-tuple-element.126), channel_id=1, source_target_pairs={{0,16},{4,20},{8,24},{12,28},{16,0},{20,4},{24,8},{28,12},{1,17},{... | collective-permute-start | bytes 294920 | tf_op jit(solution)/shard_map/ppermute | solution.py:411
  172.9 4.5 %collective-permute-start.25 = (bf16[24,2048]{1,0:T(8,128)(2,1)S(1)}, bf16[24,2048]{1,0:T(8,128)(2,1)S(1)}, u32[]{:S(2)}, u32[]{:S(2)}) collective-permute-start(bf16[24,2048]{1,0:T(8,128)(2,1)S(1)} %get-tuple-element.125), channel_id=1, source_target_pairs={{0,20},{4,16},{8,28},{12,24},{16,4},{20,0},{24,12},{28,8},{1,21},{... | collective-permute-start | bytes 294920 | tf_op jit(solution)/shard_map/ppermute | solution.py:411
  177.4 5.4 %collective-permute-start.26 = (bf16[24,2048]{1,0:T(8,128)(2,1)S(1)}, bf16[24,2048]{1,0:T(8,128)(2,1)S(1)}, u32[]{:S(2)}, u32[]{:S(2)}) collective-permute-start(bf16[24,2048]{1,0:T(8,128)(2,1)S(1)} %get-tuple-element.124), channel_id=1, source_target_pairs={{0,24},{4,28},{8,16},{12,20},{16,8},{20,12},{24,0},{28,4},{1,25},{... | collective-permute-start | bytes 294920 | tf_op jit(solution)/shard_map/ppermute | solution.py:411
  182.8 2.2 %collective-permute-start.27 = (bf16[24,2048]{1,0:T(8,128)(2,1)S(1)}, bf16[24,2048]{1,0:T(8,128)(2,1)S(1)}, u32[]{:S(2)}, u32[]{:S(2)}) collective-permute-start(bf16[24,2048]{1,0:T(8,128)(2,1)S(1)} %get-tuple-element.123), channel_id=1, source_target_pairs={{0,28},{4,24},{8,20},{12,16},{16,12},{20,8},{24,4},{28,0},{1,29},{... | collective-permute-start | bytes 294920 | tf_op jit(solution)/shard_map/ppermute | solution.py:411
  186.5 3.6 %collective-permute-done.27.refs_7_ = bf16[24,2048]{1,0:T(8,128)(2,1)S(1)} collective-permute-done((bf16[24,2048]{1,0:T(8,128)(2,1)S(1)}, bf16[24,2048]{1,0:T(8,128)(2,1)S(1)}, u32[]{:S(2)}, u32[]{:S(2)}) %collective-permute-start.27) | collective-permute-done | bytes 98336 | tf_op jit(solution)/shard_map/ppermute | solution.py:411
  (145 shorter events, 58.3 us)
Async XLA Ops:
  17.9 17.2 %collective-permute-start.5 = (bf16[288,192]{1,0:T(8,128)(2,1)S(1)}, bf16[288,192]{1,0:T(8,128)(2,1)S(1)}, u32[]{:S(2)}, u32[]{:S(2)}) collective-permute-start(bf16[288,192]{1,0:T(8,128)(2,1)S(1)} %get-tuple-element.64), channel_id=1, source_target_pairs={{0,1},{1,0},{2,3},{3,2},{4,5},{5,4},{6,7},{7,6},{8,9},{9,8},{10,11... | collective-permute-start | bytes 331784 | tf_op jit(solution)/shard_map/ppermute | solution.py:402
  18.0 18.2 %collective-permute-start.6 = (bf16[288,192]{1,0:T(8,128)(2,1)S(1)}, bf16[288,192]{1,0:T(8,128)(2,1)S(1)}, u32[]{:S(2)}, u32[]{:S(2)}) collective-permute-start(bf16[288,192]{1,0:T(8,128)(2,1)S(1)} %get-tuple-element.65), channel_id=1, source_target_pairs={{0,2},{1,3},{2,0},{3,1},{4,6},{5,7},{6,4},{7,5},{8,10},{9,11},{10,... | collective-permute-start | bytes 331784 | tf_op jit(solution)/shard_map/ppermute | solution.py:402
  19.6 16.6 %collective-permute-start.7 = (bf16[288,192]{1,0:T(8,128)(2,1)S(1)}, bf16[288,192]{1,0:T(8,128)(2,1)S(1)}, u32[]{:S(2)}, u32[]{:S(2)}) collective-permute-start(bf16[288,192]{1,0:T(8,128)(2,1)S(1)} %get-tuple-element.66), channel_id=1, source_target_pairs={{0,3},{1,2},{2,1},{3,0},{4,7},{5,6},{6,5},{7,4},{8,11},{9,10},{10,... | collective-permute-start | bytes 331784 | tf_op jit(solution)/shard_map/ppermute | solution.py:402
  30.2 13.0 %collective-permute-start.32 = (bf16[24,2048]{1,0:T(8,128)(2,1)S(1)}, bf16[24,2048]{1,0:T(8,128)(2,1)S(1)}, u32[]{:S(2)}, u32[]{:S(2)}) collective-permute-start(bf16[24,2048]{1,0:T(8,128)(2,1)S(1)} %get-tuple-element.92), channel_id=1, source_target_pairs={{0,16},{4,20},{8,24},{12,28},{16,0},{20,4},{24,8},{28,12},{1,17},{... | collective-permute-start | bytes 294920 | tf_op jit(solution)/shard_map/ppermute | solution.py:411
  32.9 14.6 %collective-permute-start.33 = (bf16[24,2048]{1,0:T(8,128)(2,1)S(1)}, bf16[24,2048]{1,0:T(8,128)(2,1)S(1)}, u32[]{:S(2)}, u32[]{:S(2)}) collective-permute-start(bf16[24,2048]{1,0:T(8,128)(2,1)S(1)} %get-tuple-element.93), channel_id=1, source_target_pairs={{0,20},{4,16},{8,28},{12,24},{16,4},{20,0},{24,12},{28,8},{1,21},{... | collective-permute-start | bytes 294920 | tf_op jit(solution)/shard_map/ppermute | solution.py:411
  35.1 12.4 %collective-permute-start.34 = (bf16[24,2048]{1,0:T(8,128)(2,1)S(1)}, bf16[24,2048]{1,0:T(8,128)(2,1)S(1)}, u32[]{:S(2)}, u32[]{:S(2)}) collective-permute-start(bf16[24,2048]{1,0:T(8,128)(2,1)S(1)} %get-tuple-element.94), channel_id=1, source_target_pairs={{0,24},{4,28},{8,16},{12,20},{16,8},{20,12},{24,0},{28,4},{1,25},{... | collective-permute-start | bytes 294920 | tf_op jit(solution)/shard_map/ppermute | solution.py:411
  38.0 25.8 %collective-permute-start.10 = (bf16[48,2048]{1,0:T(8,128)(2,1)S(1)}, bf16[48,2048]{1,0:T(8,128)(2,1)S(1)}, u32[]{:S(2)}, u32[]{:S(2)}) collective-permute-start(bf16[48,2048]{1,0:T(8,128)(2,1)S(1)} %get-tuple-element.72), channel_id=1, source_target_pairs={{0,12},{4,8},{8,4},{12,0},{16,28},{20,24},{24,20},{28,16},{1,13},{... | collective-permute-start | bytes 589832 | tf_op jit(solution)/shard_map/ppermute | solution.py:411
  39.1 12.9 %collective-permute-start.35 = (bf16[24,2048]{1,0:T(8,128)(2,1)S(1)}, bf16[24,2048]{1,0:T(8,128)(2,1)S(1)}, u32[]{:S(2)}, u32[]{:S(2)}) collective-permute-start(bf16[24,2048]{1,0:T(8,128)(2,1)S(1)} %get-tuple-element.95), channel_id=1, source_target_pairs={{0,28},{4,24},{8,20},{12,16},{16,12},{20,8},{24,4},{28,0},{1,29},{... | collective-permute-start | bytes 294920 | tf_op jit(solution)/shard_map/ppermute | solution.py:411
  43.3 14.1 %collective-permute-start.28 = (bf16[24,2048]{1,0:T(8,128)(2,1)S(1)}, bf16[24,2048]{1,0:T(8,128)(2,1)S(1)}, u32[]{:S(2)}, u32[]{:S(2)}) collective-permute-start(bf16[24,2048]{1,0:T(8,128)(2,1)S(1)} %get-tuple-element.89), channel_id=1, source_target_pairs={{0,4},{4,0},{8,12},{12,8},{16,20},{20,16},{24,28},{28,24},{1,5},{5... | collective-permute-start | bytes 294920 | tf_op jit(solution)/shard_map/ppermute | solution.py:411
  47.5 13.5 %collective-permute-start.30 = (bf16[24,2048]{1,0:T(8,128)(2,1)S(1)}, bf16[24,2048]{1,0:T(8,128)(2,1)S(1)}, u32[]{:S(2)}, u32[]{:S(2)}) collective-permute-start(bf16[24,2048]{1,0:T(8,128)(2,1)S(1)} %get-tuple-element.91), channel_id=1, source_target_pairs={{0,12},{4,8},{8,4},{12,0},{16,28},{20,24},{24,20},{28,16},{1,13},{... | collective-permute-start | bytes 294920 | tf_op jit(solution)/shard_map/ppermute | solution.py:411
  52.0 24.6 %collective-permute-start.11 = (bf16[48,2048]{1,0:T(8,128)(2,1)S(1)}, bf16[48,2048]{1,0:T(8,128)(2,1)S(1)}, u32[]{:S(2)}, u32[]{:S(2)}) collective-permute-start(bf16[48,2048]{1,0:T(8,128)(2,1)S(1)} %get-tuple-element.73), channel_id=1, source_target_pairs={{0,16},{4,20},{8,24},{12,28},{16,0},{20,4},{24,8},{28,12},{1,17},{... | collective-permute-start | bytes 589832 | tf_op jit(solution)/shard_map/ppermute | solution.py:411
  57.4 24.2 %collective-permute-start.12 = (bf16[48,2048]{1,0:T(8,128)(2,1)S(1)}, bf16[48,2048]{1,0:T(8,128)(2,1)S(1)}, u32[]{:S(2)}, u32[]{:S(2)}) collective-permute-start(bf16[48,2048]{1,0:T(8,128)(2,1)S(1)} %get-tuple-element.74), channel_id=1, source_target_pairs={{0,20},{4,16},{8,28},{12,24},{16,4},{20,0},{24,12},{28,8},{1,21},{... | collective-permute-start | bytes 589832 | tf_op jit(solution)/shard_map/ppermute | solution.py:411
  59.6 22.7 %collective-permute-start.13 = (bf16[48,2048]{1,0:T(8,128)(2,1)S(1)}, bf16[48,2048]{1,0:T(8,128)(2,1)S(1)}, u32[]{:S(2)}, u32[]{:S(2)}) collective-permute-start(bf16[48,2048]{1,0:T(8,128)(2,1)S(1)} %get-tuple-element.75), channel_id=1, source_target_pairs={{0,24},{4,28},{8,16},{12,20},{16,8},{20,12},{24,0},{28,4},{1,25},{... | collective-permute-start | bytes 589832 | tf_op jit(solution)/shard_map/ppermute | solution.py:411
  61.0 24.7 %collective-permute-start.14 = (bf16[48,2048]{1,0:T(8,128)(2,1)S(1)}, bf16[48,2048]{1,0:T(8,128)(2,1)S(1)}, u32[]{:S(2)}, u32[]{:S(2)}) collective-permute-start(bf16[48,2048]{1,0:T(8,128)(2,1)S(1)} %get-tuple-element.76), channel_id=1, source_target_pairs={{0,28},{4,24},{8,20},{12,16},{16,12},{20,8},{24,4},{28,0},{1,29},{... | collective-permute-start | bytes 589832 | tf_op jit(solution)/shard_map/ppermute | solution.py:411
  63.8 27.0 %collective-permute-start.43 = (bf16[96,2048]{1,0:T(8,128)(2,1)S(1)}, bf16[96,2048]{1,0:T(8,128)(2,1)S(1)}, u32[]{:S(2)}, u32[]{:S(2)}) collective-permute-start(bf16[96,2048]{1,0:T(8,128)(2,1)S(1)} %shard_map.221.refs_3_), channel_id=1, source_target_pairs={{0,2},{1,3},{2,0},{3,1},{4,6},{5,7},{6,4},{7,5},{8,10},{9,11},{10,... | collective-permute-start | bytes 1179656 | tf_op jit(solution)/shard_map/ppermute | solution.py:402
  76.6 24.3 %collective-permute-start.54 = (bf16[2,96,2048]{2,1,0:T(8,128)(2,1)S(1)}, bf16[2,96,2048]{2,1,0:T(8,128)(2,1)S(1)}, u32[]{:S(2)}, u32[]{:S(2)}) collective-permute-start(bf16[2,96,2048]{2,1,0:T(8,128)(2,1)S(1)} %get-tuple-element.110), channel_id=1, source_target_pairs={{0,1},{1,0},{2,3},{3,2},{4,5},{5,4},{6,7},{7,6},{8,9},{9,8},{10,11... | collective-permute-start | bytes 2359304 | tf_op jit(solution)/shard_map/ppermute | solution.py:402
  90.9 12.4 %collective-permute-start.15 = (bf16[192,2048]{1,0:T(8,128)(2,1)S(1)}, bf16[192,2048]{1,0:T(8,128)(2,1)S(1)}, u32[]{:S(2)}, u32[]{:S(2)}) collective-permute-start(bf16[192,2048]{1,0:T(8,128)(2,1)S(1)} %get-tuple-element.77.refs_1_), channel_id=1, source_target_pairs={{0,1},{1,0},{2,3},{3,2},{4,5},{5,4},{6,7},{7,6},{8,9},{9,8},{10,11... | collective-permute-start | bytes 2359304 | tf_op jit(solution)/shard_map/ppermute | solution.py:402
  91.5 15.1 %collective-permute-start.17 = (bf16[192,2048]{1,0:T(8,128)(2,1)S(1)}, bf16[192,2048]{1,0:T(8,128)(2,1)S(1)}, u32[]{:S(2)}, u32[]{:S(2)}) collective-permute-start(bf16[192,2048]{1,0:T(8,128)(2,1)S(1)} %get-tuple-element.83.refs_1_), channel_id=1, source_target_pairs={{0,1},{1,0},{2,3},{3,2},{4,5},{5,4},{6,7},{7,6},{8,9},{9,8},{10,11... | collective-permute-start | bytes 2359304 | tf_op jit(solution)/shard_map/ppermute | solution.py:402
  101.5 31.6 %collective-permute-start.37 = (bf16[96,2048]{1,0:T(8,128)(2,1)S(1)}, bf16[96,2048]{1,0:T(8,128)(2,1)S(1)}, u32[]{:S(2)}, u32[]{:S(2)}) collective-permute-start(bf16[96,2048]{1,0:T(8,128)(2,1)S(1)} %get-tuple-element.97), channel_id=1, source_target_pairs={{0,1},{1,0},{2,3},{3,2},{4,5},{5,4},{6,7},{7,6},{8,9},{9,8},{10,11... | collective-permute-start | bytes 1179656 | tf_op jit(solution)/shard_map/ppermute | solution.py:402
  103.4 53.9 %collective-permute-start.55 = (bf16[96,2048]{1,0:T(8,128)(2,1)S(1)}, bf16[96,2048]{1,0:T(8,128)(2,1)S(1)}, u32[]{:S(2)}, u32[]{:S(2)}) collective-permute-start(bf16[96,2048]{1,0:T(8,128)(2,1)S(1)} %get-tuple-element.111), channel_id=1, source_target_pairs={{0,2},{1,3},{2,0},{3,1},{4,6},{5,7},{6,4},{7,5},{8,10},{9,11},{10,... | collective-permute-start | bytes 1179656 | tf_op jit(solution)/shard_map/ppermute | solution.py:402
  108.3 29.7 %collective-permute-start.16 = (bf16[192,2048]{1,0:T(8,128)(2,1)S(1)}, bf16[192,2048]{1,0:T(8,128)(2,1)S(1)}, u32[]{:S(2)}, u32[]{:S(2)}) collective-permute-start(bf16[192,2048]{1,0:T(8,128)(2,1)S(1)} %get-tuple-element.82), channel_id=1, source_target_pairs={{0,1},{1,0},{2,3},{3,2},{4,5},{5,4},{6,7},{7,6},{8,9},{9,8},{10,11... | collective-permute-start | bytes 2359304 | tf_op jit(solution)/shard_map/ppermute | solution.py:402
  109.0 13.9 %collective-permute-start.46 = (bf16[96,2048]{1,0:T(8,128)(2,1)S(1)}, bf16[96,2048]{1,0:T(8,128)(2,1)S(1)}, u32[]{:S(2)}, u32[]{:S(2)}) collective-permute-start(bf16[96,2048]{1,0:T(8,128)(2,1)S(1)} %add_convert_fusion.6), channel_id=1, source_target_pairs={{0,2},{1,3},{2,0},{3,1},{4,6},{5,7},{6,4},{7,5},{8,10},{9,11},{10,... | collective-permute-start | bytes 1179656 | tf_op jit(solution)/shard_map/ppermute | solution.py:402
  109.7 27.1 %collective-permute-start.18 = (bf16[192,2048]{1,0:T(8,128)(2,1)S(1)}, bf16[192,2048]{1,0:T(8,128)(2,1)S(1)}, u32[]{:S(2)}, u32[]{:S(2)}) collective-permute-start(bf16[192,2048]{1,0:T(8,128)(2,1)S(1)} %get-tuple-element.85), channel_id=1, source_target_pairs={{0,1},{1,0},{2,3},{3,2},{4,5},{5,4},{6,7},{7,6},{8,9},{9,8},{10,11... | collective-permute-start | bytes 2359304 | tf_op jit(solution)/shard_map/ppermute | solution.py:402
  133.3 25.3 %collective-permute-start.47 = (bf16[24,2048]{1,0:T(8,128)(2,1)S(1)}, bf16[24,2048]{1,0:T(8,128)(2,1)S(1)}, u32[]{:S(2)}, u32[]{:S(2)}) collective-permute-start(bf16[24,2048]{1,0:T(8,128)(2,1)S(1)} %get-tuple-element.121), channel_id=1, source_target_pairs={{0,4},{4,0},{8,12},{12,8},{16,20},{20,16},{24,28},{28,24},{1,5},{5... | collective-permute-start | bytes 294920 | tf_op jit(solution)/shard_map/ppermute | solution.py:411
  134.9 25.9 %collective-permute-start.48 = (bf16[24,2048]{1,0:T(8,128)(2,1)S(1)}, bf16[24,2048]{1,0:T(8,128)(2,1)S(1)}, u32[]{:S(2)}, u32[]{:S(2)}) collective-permute-start(bf16[24,2048]{1,0:T(8,128)(2,1)S(1)} %get-tuple-element.120), channel_id=1, source_target_pairs={{0,8},{4,12},{8,0},{12,4},{16,24},{20,28},{24,16},{28,20},{1,9},{5... | collective-permute-start | bytes 294920 | tf_op jit(solution)/shard_map/ppermute | solution.py:411
  136.7 26.4 %collective-permute-start.49 = (bf16[24,2048]{1,0:T(8,128)(2,1)S(1)}, bf16[24,2048]{1,0:T(8,128)(2,1)S(1)}, u32[]{:S(2)}, u32[]{:S(2)}) collective-permute-start(bf16[24,2048]{1,0:T(8,128)(2,1)S(1)} %get-tuple-element.119), channel_id=1, source_target_pairs={{0,12},{4,8},{8,4},{12,0},{16,28},{20,24},{24,20},{28,16},{1,13},{... | collective-permute-start | bytes 294920 | tf_op jit(solution)/shard_map/ppermute | solution.py:411
  157.3 13.6 %collective-permute-start.51 = (bf16[24,2048]{1,0:T(8,128)(2,1)S(1)}, bf16[24,2048]{1,0:T(8,128)(2,1)S(1)}, u32[]{:S(2)}, u32[]{:S(2)}) collective-permute-start(bf16[24,2048]{1,0:T(8,128)(2,1)S(1)} %get-tuple-element.117), channel_id=1, source_target_pairs={{0,20},{4,16},{8,28},{12,24},{16,4},{20,0},{24,12},{28,8},{1,21},{... | collective-permute-start | bytes 294920 | tf_op jit(solution)/shard_map/ppermute | solution.py:411
  163.1 14.2 %collective-permute-start.21 = (bf16[24,2048]{1,0:T(8,128)(2,1)S(1)}, bf16[24,2048]{1,0:T(8,128)(2,1)S(1)}, u32[]{:S(2)}, u32[]{:S(2)}) collective-permute-start(bf16[24,2048]{1,0:T(8,128)(2,1)S(1)} %get-tuple-element.129), channel_id=1, source_target_pairs={{0,4},{4,0},{8,12},{12,8},{16,20},{20,16},{24,28},{28,24},{1,5},{5... | collective-permute-start | bytes 294920 | tf_op jit(solution)/shard_map/ppermute | solution.py:411
  165.9 16.9 %collective-permute-start.22 = (bf16[24,2048]{1,0:T(8,128)(2,1)S(1)}, bf16[24,2048]{1,0:T(8,128)(2,1)S(1)}, u32[]{:S(2)}, u32[]{:S(2)}) collective-permute-start(bf16[24,2048]{1,0:T(8,128)(2,1)S(1)} %get-tuple-element.128), channel_id=1, source_target_pairs={{0,8},{4,12},{8,0},{12,4},{16,24},{20,28},{24,16},{28,20},{1,9},{5... | collective-permute-start | bytes 294920 | tf_op jit(solution)/shard_map/ppermute | solution.py:411
  170.9 15.0 %collective-permute-start.23 = (bf16[24,2048]{1,0:T(8,128)(2,1)S(1)}, bf16[24,2048]{1,0:T(8,128)(2,1)S(1)}, u32[]{:S(2)}, u32[]{:S(2)}) collective-permute-start(bf16[24,2048]{1,0:T(8,128)(2,1)S(1)} %get-tuple-element.127), channel_id=1, source_target_pairs={{0,12},{4,8},{8,4},{12,0},{16,28},{20,24},{24,20},{28,16},{1,13},{... | collective-permute-start | bytes 294920 | tf_op jit(solution)/shard_map/ppermute | solution.py:411
  170.9 15.0 %collective-permute-start.24 = (bf16[24,2048]{1,0:T(8,128)(2,1)S(1)}, bf16[24,2048]{1,0:T(8,128)(2,1)S(1)}, u32[]{:S(2)}, u32[]{:S(2)}) collective-permute-start(bf16[24,2048]{1,0:T(8,128)(2,1)S(1)} %get-tuple-element.126), channel_id=1, source_target_pairs={{0,16},{4,20},{8,24},{12,28},{16,0},{20,4},{24,8},{28,12},{1,17},{... | collective-permute-start | bytes 294920 | tf_op jit(solution)/shard_map/ppermute | solution.py:411
  172.9 13.1 %collective-permute-start.25 = (bf16[24,2048]{1,0:T(8,128)(2,1)S(1)}, bf16[24,2048]{1,0:T(8,128)(2,1)S(1)}, u32[]{:S(2)}, u32[]{:S(2)}) collective-permute-start(bf16[24,2048]{1,0:T(8,128)(2,1)S(1)} %get-tuple-element.125), channel_id=1, source_target_pairs={{0,20},{4,16},{8,28},{12,24},{16,4},{20,0},{24,12},{28,8},{1,21},{... | collective-permute-start | bytes 294920 | tf_op jit(solution)/shard_map/ppermute | solution.py:411
  (38 other events, 353.6 us)
